TPU v7x, 128 devices: a whole 4x4x4 slice. The times are simulated.
128 devices in a mesh: fs: 16 (over z, x), tp: 8 (over y, core).
Axes of the slice: x: 4, y: 4, z: 4, core: 2. Of those that a mesh axis runs over, the one named last changes fastest.
Arguments:
- normed_input: bfloat16 [32768, 2048], P('fs'), may hold values from -6 to 6
- forget_cot: bfloat16 [32768, 2048], P('fs', 'tp'), may hold values from -6 to 6
- value_cot: bfloat16 [32768, 2048], P('fs', 'tp'), may hold values from -6 to 6
- gated_output: bfloat16 [32768, 2048], P('fs', 'tp'), may hold values from -6 to 6
- output_cot: bfloat16 [32768, 2048], P('fs'), may hold values from -6 to 6
- forget_weight: float32 [2048, 2048], P('fs', 'tp'), may hold values from -0.125 to 0.125
- value_weight: float32 [2048, 2048], P('fs', 'tp'), may hold values from -0.125 to 0.125
- out_weight: float32 [2048, 2048], P('tp', 'fs'), may hold values from -0.125 to 0.125
- bases: bfloat16 [3, 2048, 256], replicated, may hold values from -0.125 to 0.125
- first_moment: float32 [256, 3, 2048], P('fs', None, 'tp'), may hold values from -4 to 4
- second_moment: float32 [256, 3, 2048], P('fs', None, 'tp'), may hold values from 0.25 to 4
Outputs:
- new_forget: float32 [2048, 2048], P('fs', 'tp')
- new_value: float32 [2048, 2048], P('fs', 'tp')
- new_out: float32 [2048, 2048], P('tp', 'fs')
- copy_forget: bfloat16 [2048, 2048], P(None, 'tp')
- copy_value: bfloat16 [2048, 2048], P(None, 'tp')
- copy_out: bfloat16 [2048, 2048], P('tp')
- moment_one: float32 [256, 3, 2048], P('fs', None, 'tp')
- moment_two: float32 [256, 3, 2048], P('fs', None, 'tp')
- step_forget: float32 [2048, 2048], P('fs', 'tp')
- step_value: float32 [2048, 2048], P('fs', 'tp')
- step_out: float32 [2048, 2048], P('tp', 'fs')
All inputs are finite; a program needn't handle non-finite values.
Results may differ from a plain program's by a relative error of at most 0.0045.
Values may be sent and summed in bfloat16 or wider, within the bound.
A program may use at most 128 MiB of HBM per device.

v0:
```python
import functools

import jax
import jax.numpy as jnp
from jax import lax
from jax.experimental import pallas as pl
from jax.experimental.pallas import tpu as pltpu
from jax.sharding import PartitionSpec as P

MESH = pl.DeviceIdType.MESH


def ring_index(place, size):
    back = lax.div(place, size // 2)
    return (1 - back) * 2 * place + back * (2 * (size - 1 - place) + 1)


def ring_place(index, size):
    odd = lax.rem(index, 2)
    half = lax.div(index, 2)
    return (1 - odd) * half + odd * (size - 1 - half)


def exchange_kernel(
    size,
    groups,
    factor,
    entries,
    x_hbm,
    oc_hbm,
    fc_hbm,
    vc_hbm,
    go_hbm,
    bases_hbm,
    fw_hbm,
    vw_hbm,
    ow_hbm,
    m1_hbm,
    m2_hbm,
    all_f,
    all_v,
    all_o,
    dirs_out,
    scale_ref,
    n1_ref,
    n2_ref,
    fw_ref,
    vw_ref,
    ow_ref,
    m1_ref,
    m2_ref,
    first_sem,
    x_buf,
    oc_buf,
    c_buf,
    b_buf,
    wf_buf,
    wv_buf,
    wo_buf,
    acc,
    part,
    got,
    mine,
    dirs,
    sums,
    load_sem,
    base_sem,
    put_sem,
    ring_send,
    ring_recv,
    part_send,
    part_recv,
    dir_send,
    dir_recv,
    sum_send,
    sum_recv,
):
    me = lax.axis_index("fs")
    mt = lax.axis_index("tp")
    place = ring_place(me, size)
    right = ring_index(lax.rem(place + 1, size), size)
    left = ring_index(lax.rem(place + size - 1, size), size)
    steps = size // 2
    tiles = load_sem.shape[1]
    tokens = x_buf.shape[0]
    rows_t = tokens // tiles
    rank_rows = m1_ref.shape[1]
    columns = m1_ref.shape[2]

    firsts = [
        pltpu.make_async_copy(src, dst, first_sem.at[i])
        for i, (src, dst) in enumerate(
            (
                (fw_hbm, fw_ref),
                (vw_hbm, vw_ref),
                (ow_hbm, ow_ref),
                (m1_hbm, m1_ref),
                (m2_hbm, m2_ref),
            )
        )
    ]
    for copy in firsts[:3]:
        copy.start()
    base_copies = [
        pltpu.make_async_copy(bases_hbm.at[k], b_buf.at[k], base_sem.at[k]) for k in range(3)
    ]

    def load(which, src, dst, tile):
        at = pl.ds(pl.multiple_of(tile * rows_t, rows_t), rows_t)
        return pltpu.make_async_copy(src.at[at, :], dst.at[at, :], load_sem.at[which, tile])

    streams = (
        (x_hbm, x_buf),
        (fc_hbm, c_buf.at[0]),
        (vc_hbm, c_buf.at[1]),
        (oc_hbm, oc_buf),
        (go_hbm, c_buf.at[2]),
    )
    base_copies[0].start()
    for tile in range(tiles):
        for which in (0, 1):
            load(which, *streams[which], tile).start()
    base_copies[1].start()
    for tile in range(tiles):
        load(2, *streams[2], tile).start()
    base_copies[2].start()
    for tile in range(tiles):
        for which in (3, 4):
            load(which, *streams[which], tile).start()

    for copy in firsts[3:]:
        copy.start()

    barrier = pltpu.get_barrier_semaphore()
    for j in range(1, size):
        pl.semaphore_signal(
            barrier, inc=1, device_id=(lax.rem(me + j, size), mt), device_id_type=MESH
        )
    for j in range(1, groups):
        pl.semaphore_signal(
            barrier, inc=1, device_id=(me, lax.rem(mt + j, groups)), device_id_type=MESH
        )
    for copy in firsts[:3]:
        copy.wait()
    wf_buf[...] = fw_ref[...].astype(jnp.bfloat16)
    wv_buf[...] = vw_ref[...].astype(jnp.bfloat16)
    wo_buf[...] = ow_ref[...].astype(jnp.bfloat16)
    pl.semaphore_wait(barrier, size - 1 + groups - 1)

    def row_block(ref, owner, half):
        rows = wf_buf.shape[0]
        start, count = owner * rows, rows
        if half is not None:
            count = rows // 2
            start = start + half * count
        return ref.at[pl.ds(pl.multiple_of(start, count), count), :]

    def column_block(ref, owner, half):
        width = wo_buf.shape[1]
        lanes = pl.ds(pl.multiple_of(owner * width, width), width)
        height = wo_buf.shape[0]
        if half is None:
            return ref.at[:, lanes]
        return ref.at[pl.ds(half * (height // 2), height // 2), lanes]

    def dir_block(k, owner, half):
        at = pl.ds(pl.multiple_of(owner * rank_rows, rank_rows), rank_rows)
        if half is None:
            return dirs.at[k, at, :]
        return dirs.at[k, at, pl.ds(half * (columns // 2), columns // 2)]

    items = (
        (wf_buf, functools.partial(row_block, all_f)),
        (wv_buf, functools.partial(row_block, all_v)),
        (wo_buf, functools.partial(column_block, all_o)),
    )

    def hop(view, own, send_sem, recv_sem, item, step, way):
        sign = 1 if way == 0 else size - 1
        owner = ring_index(lax.rem(place + (size - sign) * (step - 1), size), size)
        half = way if step == steps else None
        dst = view(owner, half)
        src = own if own is not None and step == 1 and half is None else dst
        return pltpu.make_async_remote_copy(
            src_ref=src,
            dst_ref=dst,
            send_sem=send_sem.at[way, item, step - 1],
            recv_sem=recv_sem.at[way, item, step - 1],
            device_id=(right if way == 0 else left, mt),
            device_id_type=MESH,
        )

    def weight_hop(item, step, way):
        own, view = items[item]
        return hop(view, own, ring_send, ring_recv, item, step, way)

    def dir_hop(k, step, way):
        own = mine.at[k]
        return hop(functools.partial(dir_block, k), own, dir_send, dir_recv, k, step, way)

    puts = []
    for item in range(3):
        own, view = items[item]
        put = pltpu.make_async_copy(own, view(me, None), put_sem.at[item])
        put.start()
        puts.append(put)
        for way in range(2):
            weight_hop(item, 1, way).start()

    forwards = [(step, item) for step in range(2, steps + 1) for item in range(3)]

    def pump(count):
        for _ in range(min(count, len(forwards))):
            step, item = forwards.pop(0)
            for way in range(2):
                weight_hop(item, step - 1, way).wait_recv()
                weight_hop(item, step, way).start()

    def part_copy(k, j):
        owner = lax.rem(me + j, size)
        at = pl.ds(pl.multiple_of(owner * rank_rows, rank_rows), rank_rows)
        return pltpu.make_async_remote_copy(
            src_ref=part.at[k, at, :],
            dst_ref=got.at[k, j - 1],
            send_sem=part_send.at[k, j - 1],
            recv_sem=part_recv.at[k, j - 1],
            device_id=(owner, mt),
            device_id_type=MESH,
        )

    own_rows = pl.ds(pl.multiple_of(me * rank_rows, rank_rows), rank_rows)

    def combine(k):
        projected = acc[k, own_rows, :] * factor
        for j in range(1, size):
            part_copy(k, j).wait_recv()
            projected = projected + got[k, j - 1].astype(jnp.float32)
        one = 0.9 * m1_ref[k] + 0.1 * projected
        two = 0.9 * m2_ref[k] + 0.1 * projected * projected
        n1_ref[k] = one
        n2_ref[k] = two
        rounded = (one / (jnp.sqrt(two) + 1e-08)).astype(jnp.bfloat16)
        mine[k] = rounded
        dirs[k, own_rows, :] = rounded
        for way in range(2):
            dir_hop(k, 1, way).start()

    for k in range(3):
        base_copies[k].wait()
        left_which, right_which = ((0, 1), (0, 2), (3, 4))[k]
        source = x_buf if k < 2 else oc_buf
        acc[k] = jnp.zeros(acc.shape[1:], acc.dtype)

        def tile_body(tile, carry, k=k, left_which=left_which, right_which=right_which, source=source):
            at = pl.ds(pl.multiple_of(tile * rows_t, rows_t), rows_t)
            if k != 1:
                load(left_which, *streams[left_which], tile).wait()
            reduced = jnp.dot(
                source[at, :], b_buf[k], preferred_element_type=jnp.float32
            ).astype(jnp.bfloat16)
            load(right_which, *streams[right_which], tile).wait()
            acc[k] += lax.dot_general(
                reduced,
                c_buf[k, at, :],
                (((0,), (0,)), ((), ())),
                preferred_element_type=jnp.float32,
            )
            return carry

        lax.fori_loop(0, tiles, tile_body, 0)
        part[k] = (acc[k] * factor).astype(jnp.bfloat16)
        for j in range(1, size):
            part_copy(k, j).start()
        pump(1)
        if k == 1:
            for copy in firsts[3:]:
                copy.wait()
        if k > 0:
            combine(k - 1)

    pump(1)
    combine(2)
    pump(2)
    for step in range(2, steps + 1):
        for k in range(3):
            for way in range(2):
                dir_hop(k, step - 1, way).wait_recv()
                dir_hop(k, step, way).start()
        if step == 3:
            pump(3)
    pump(len(forwards))
    for k in range(3):
        for way in range(2):
            dir_hop(k, steps, way).wait_recv()

    dirs_put = pltpu.make_async_copy(dirs, dirs_out, put_sem.at[3])
    dirs_put.start()

    row = lax.broadcasted_iota(jnp.int32, scale_ref.shape, 0)
    tile_sum = jnp.zeros(scale_ref.shape, jnp.float32)
    for k in range(3):
        values = dirs[k].astype(jnp.float32)
        tile_sum = tile_sum + jnp.where(row == k, jnp.sum(values * values), 0.0)
    sums[0] = tile_sum

    def sum_copy(j):
        return pltpu.make_async_remote_copy(
            src_ref=sums.at[0],
            dst_ref=sums.at[j],
            send_sem=sum_send.at[j],
            recv_sem=sum_recv.at[j],
            device_id=(me, lax.rem(mt + j, groups)),
            device_id_type=MESH,
        )

    for j in range(1, groups):
        sum_copy(j).start()
    total = tile_sum
    for j in range(1, groups):
        sum_copy(j).wait_recv()
        total = total + sums[j]
    scale_ref[...] = lax.rsqrt(total / entries + 1.0)

    for item in range(3):
        for way in range(2):
            weight_hop(item, steps, way).wait_recv()
    for put in puts:
        put.wait()
    dirs_put.wait()
    for k in range(3):
        for step in range(1, steps + 1):
            for way in range(2):
                weight_hop(k, step, way).wait_send()
                dir_hop(k, step, way).wait_send()
        for j in range(1, size):
            part_copy(k, j).wait_send()
    for j in range(1, groups):
        sum_copy(j).wait_send()


def exchange(size, groups, x, oc, fc, vc, go, bases, fw, vw, ow, m1, m2):
    tokens, width = x.shape
    rank = bases.shape[2]
    rows, columns = fw.shape
    rank_rows = m1.shape[1]
    steps = size // 2
    tiles = 4
    bf16, f32 = jnp.bfloat16, jnp.float32
    hbm = pl.BlockSpec(memory_space=pl.ANY)
    vmem = pl.BlockSpec(memory_space=pltpu.VMEM)
    dma = pltpu.SemaphoreType.DMA
    kernel = functools.partial(
        exchange_kernel,
        size,
        groups,
        float(tokens * size) ** (-0.5),
        float(rank * columns * groups),
    )
    return pl.pallas_call(
        kernel,
        out_shape=(
            jax.ShapeDtypeStruct((rows * size, columns), bf16),
            jax.ShapeDtypeStruct((rows * size, columns), bf16),
            jax.ShapeDtypeStruct((ow.shape[0], ow.shape[1] * size), bf16),
            jax.ShapeDtypeStruct((3, rank, columns), bf16),
            jax.ShapeDtypeStruct((8, 128), f32),
            jax.ShapeDtypeStruct(m1.shape, f32),
            jax.ShapeDtypeStruct(m2.shape, f32),
        ),
        in_specs=[pl.BlockSpec(memory_space=pltpu.HBM)] * 11,
        out_specs=(hbm,) * 4 + (vmem,) * 3,
        scratch_shapes=[
            pltpu.VMEM(fw.shape, f32),
            pltpu.VMEM(vw.shape, f32),
            pltpu.VMEM(ow.shape, f32),
            pltpu.VMEM(m1.shape, f32),
            pltpu.VMEM(m2.shape, f32),
            dma((5,)),
            pltpu.VMEM(x.shape, bf16),
            pltpu.VMEM(oc.shape, bf16),
            pltpu.VMEM((3, tokens, columns), bf16),
            pltpu.VMEM(bases.shape, bf16),
            pltpu.VMEM(fw.shape, bf16),
            pltpu.VMEM(vw.shape, bf16),
            pltpu.VMEM(ow.shape, bf16),
            pltpu.VMEM((3, rank, columns), f32),
            pltpu.VMEM((3, rank, columns), bf16),
            pltpu.VMEM((3, size - 1, rank_rows, columns), bf16),
            pltpu.VMEM((3, rank_rows, columns), bf16),
            pltpu.VMEM((3, rank, columns), bf16),
            pltpu.VMEM((groups, 8, 128), f32),
            dma((5, tiles)),
            dma((3,)),
            dma((4,)),
            dma((2, 3, steps)),
            dma((2, 3, steps)),
            dma((3, size - 1)),
            dma((3, size - 1)),
            dma((2, 3, steps)),
            dma((2, 3, steps)),
            dma((groups,)),
            dma((groups,)),
        ],
        compiler_params=pltpu.CompilerParams(
            collective_id=0, has_side_effects=True, vmem_limit_bytes=54 * 1024 * 1024
        ),
    )(x, oc, fc, vc, go, bases, fw, vw, ow, m1, m2)


def finish_kernel(
    scale_hbm,
    dirs_hbm,
    f_hbm,
    v_hbm,
    o_hbm,
    n1_hbm,
    n2_hbm,
    bases_hbm,
    fw_hbm,
    vw_hbm,
    ow_hbm,
    new_f,
    new_v,
    new_o,
    copy_f,
    copy_v,
    copy_o,
    n1_out,
    n2_out,
    step_f,
    step_v,
    step_o,
    scale_ref,
    dirs_ref,
    bases_ref,
    fw_ref,
    vw_ref,
    ow_ref,
    f_ref,
    v_ref,
    o_ref,
    n1_ref,
    n2_ref,
    small_sem,
    load_sem,
    cf_buf,
    cv_buf,
    co_buf,
    down_buf,
    across_buf,
    tile_sem,
    own_sem,
):
    tiles = tile_sem.shape[1]
    rows = f_ref.shape[0] // tiles
    smalls = [
        pltpu.make_async_copy(src, dst, small_sem.at[i])
        for i, (src, dst) in enumerate(
            (
                (dirs_hbm, dirs_ref),
                (scale_hbm, scale_ref),
                (bases_hbm, bases_ref),
                (fw_hbm, fw_ref),
                (vw_hbm, vw_ref),
                (ow_hbm, ow_ref),
                (n1_hbm, n1_ref),
                (n2_hbm, n2_ref),
            )
        )
    ]
    loads = []
    for tile in range(tiles):
        at = pl.ds(tile * rows, rows)
        views = (
            (f_hbm.at[at, :], f_ref.at[at, :]),
            (v_hbm.at[at, :], v_ref.at[at, :]),
            (o_hbm.at[:, at], o_ref.at[:, at]),
        )
        loads.append(
            [
                pltpu.make_async_copy(src, dst, load_sem.at[i, tile])
                for i, (src, dst) in enumerate(views)
            ]
        )
    for copy in smalls:
        copy.start()
    for group in loads:
        for copy in group:
            copy.start()
    for copy in smalls[:6]:
        copy.wait()
    copies = []

    def put(src, dst, sem):
        copy = pltpu.make_async_copy(src, dst, sem)
        copy.start()
        copies.append(copy)

    def down(rows, k):
        step = jnp.dot(bases_ref[k, rows, :], dirs_ref[k], preferred_element_type=jnp.float32)
        return step * scale_ref[k : k + 1, 0:1]

    def across(rows):
        step = lax.dot_general(
            dirs_ref[2],
            bases_ref[2, rows, :],
            (((0,), (1,)), ((), ())),
            preferred_element_type=jnp.float32,
        )
        return step * scale_ref[2:3, 0:1]

    own = fw_ref.shape[0]
    me = pl.ds(pl.multiple_of(lax.axis_index("fs") * own, own), own)
    for k, weight, new, out in ((0, fw_ref, new_f, step_f), (1, vw_ref, new_v, step_v)):
        step = down(me, k)
        down_buf[2 * k] = step
        put(down_buf.at[2 * k], out, own_sem.at[2 * k])
        down_buf[2 * k + 1] = weight[...] - 0.01 * step
        put(down_buf.at[2 * k + 1], new, own_sem.at[2 * k + 1])
    step = across(me)
    across_buf[0] = step
    put(across_buf.at[0], step_o, own_sem.at[4])
    across_buf[1] = ow_ref[...] - 0.01 * step
    put(across_buf.at[1], new_o, own_sem.at[5])

    for copy in smalls[6:]:
        copy.wait()
    put(n1_ref, n1_out, own_sem.at[6])
    put(n2_ref, n2_out, own_sem.at[7])

    for tile in range(tiles):
        at = pl.ds(tile * rows, rows)
        for copy in loads[tile]:
            copy.wait()
        for k, old, buf, out in ((0, f_ref, cf_buf, copy_f), (1, v_ref, cv_buf, copy_v)):
            value = old[at, :].astype(jnp.float32) - 0.01 * down(at, k)
            buf[at, :] = value.astype(jnp.bfloat16)
            put(buf.at[at, :], out.at[at, :], tile_sem.at[k, tile])
        value = o_ref[:, at].astype(jnp.float32) - 0.01 * across(at)
        co_buf[:, at] = value.astype(jnp.bfloat16)
        put(co_buf.at[:, at], copy_o.at[:, at], tile_sem.at[2, tile])
    for copy in copies:
        copy.wait()


def finish(scales, dirs, bases, old_f, old_v, old_o, fw, vw, ow, one, two):
    tiles = 4
    depth, columns = old_f.shape
    rank = bases.shape[2]
    dma = pltpu.SemaphoreType.DMA
    hbm = pl.BlockSpec(memory_space=pltpu.HBM)
    outs = (fw, vw, ow, old_f, old_v, old_o, one, two, fw, vw, ow)
    return pl.pallas_call(
        finish_kernel,
        out_shape=tuple(jax.ShapeDtypeStruct(a.shape, a.dtype) for a in outs),
        in_specs=[hbm] * 11,
        out_specs=(pl.BlockSpec(memory_space=pltpu.HBM),) * 11,
        scratch_shapes=[
            pltpu.VMEM(scales.shape, jnp.float32),
            pltpu.VMEM(dirs.shape, jnp.bfloat16),
            pltpu.VMEM(bases.shape, jnp.bfloat16),
            pltpu.VMEM(fw.shape, jnp.float32),
            pltpu.VMEM(vw.shape, jnp.float32),
            pltpu.VMEM(ow.shape, jnp.float32),
            pltpu.VMEM(old_f.shape, jnp.bfloat16),
            pltpu.VMEM(old_v.shape, jnp.bfloat16),
            pltpu.VMEM(old_o.shape, jnp.bfloat16),
            pltpu.VMEM(one.shape, jnp.float32),
            pltpu.VMEM(two.shape, jnp.float32),
            dma((8,)),
            dma((3, tiles)),
            pltpu.VMEM(old_f.shape, jnp.bfloat16),
            pltpu.VMEM(old_v.shape, jnp.bfloat16),
            pltpu.VMEM(old_o.shape, jnp.bfloat16),
            pltpu.VMEM((4,) + fw.shape, jnp.float32),
            pltpu.VMEM((2,) + ow.shape, jnp.float32),
            dma((3, tiles)),
            dma((8,)),
        ],
        compiler_params=pltpu.CompilerParams(vmem_limit_bytes=56 * 1024 * 1024),
        cost_estimate=pl.CostEstimate(
            flops=6 * depth * rank * columns, bytes_accessed=16 * depth * columns, transcendentals=0
        ),
    )(scales, dirs, old_f, old_v, old_o, one, two, bases, fw, vw, ow)


def on_device(
    normed_input,
    forget_cot,
    value_cot,
    gated_output,
    output_cot,
    forget_weight,
    value_weight,
    out_weight,
    bases,
    first_moment,
    second_moment,
):
    size, groups = lax.axis_size("fs"), lax.axis_size("tp")
    old_f, old_v, old_o, dirs, scales, one, two = exchange(
        size,
        groups,
        normed_input,
        output_cot,
        forget_cot,
        value_cot,
        gated_output,
        bases,
        forget_weight,
        value_weight,
        out_weight,
        first_moment.transpose(1, 0, 2),
        second_moment.transpose(1, 0, 2),
    )
    outs = finish(
        scales,
        dirs,
        bases,
        old_f,
        old_v,
        old_o,
        forget_weight,
        value_weight,
        out_weight,
        one,
        two,
    )
    return (
        *outs[:6],
        outs[6].transpose(1, 0, 2),
        outs[7].transpose(1, 0, 2),
        *outs[8:],
    )


def solution(mesh):
    placed = (
        P("fs", None),
        P("fs", "tp"),
        P("fs", "tp"),
        P("fs", "tp"),
        P("fs", None),
        P("fs", "tp"),
        P("fs", "tp"),
        P("tp", "fs"),
        P(),
        P("fs", None, "tp"),
        P("fs", None, "tp"),
    )
    return jax.shard_map(
        on_device,
        mesh=mesh,
        in_specs=placed,
        out_specs=(
            P("fs", "tp"),
            P("fs", "tp"),
            P("tp", "fs"),
            P(None, "tp"),
            P(None, "tp"),
            P("tp", None),
            P("fs", None, "tp"),
            P("fs", None, "tp"),
            P("fs", "tp"),
            P("fs", "tp"),
            P("tp", "fs"),
        ),
        check_vma=False,
    )
```

profile of v0, /device:TPU:0, one launch (start us, length us, event | category | flops | bytes accessed | tf_op | source)
XLA Modules:
  0.0 118.4 jit_solution(839416156066154692)
XLA Ops:
  0.6 112.0 %shard_map.194 = (bf16[2048,256]{1,0:T(8,128)(2,1)}, bf16[2048,256]{1,0:T(8,128)(2,1)}, bf16[256,2048]{1,0:T(8,128)(2,1)}, bf16[3,256,256]{2,1,0:T(8,128)(2,1)},...) custom-call(bf16[2048,2048]{1,0:T(8,128)(2,1)} %x_hbm.1, bf16[2048,2048]{1,0:T(8,128)(2,1)} %oc_hbm.1, ...), custom_call_target="tpu_custom_call" | custom-call | tf_op jit(solution)/shard_map/pallas_call | solution.py:359
  112.6 5.8 %shard_map.195 = (f32[128,256]{1,0:T(8,128)}, f32[128,256]{1,0:T(8,128)}, f32[256,128]{1,0:T(8,128)}, bf16[2048,256]{1,0:T(8,128)(2,1)}, bf16[2048,256]{1,0:T(8,...) custom-call(f32[8,128]{1,0:T(8,128)} %get-tuple-element.29.scale_hbm, ...), custom_call_target="tpu_custom_call" | custom-call | flops 805306368 | bytes 8388608 | tf_op jit(solution)/shard_map/pallas_call | solution.py:553
where the time goes:
time: 120 us; the launch traced here: 118 us
  Pallas kernels  118 us (98%)
    pallas_call x1, Pallas kernels, exchange(): pl.pallas_call(kernel, out_shape=(jax.ShapeDtypeStruct((rows * size, colu...  112 us
    pallas_call x1, Pallas kernels, finish(): pl.pallas_call(finish_kernel, out_shape=tuple((jax.ShapeDtypeStruct(a.sha...  5.81 us

commit v1 on v0

v1 whole, which is shorter than its diff:
```python
import functools

import jax
import jax.numpy as jnp
from jax import lax
from jax.experimental import pallas as pl
from jax.experimental.pallas import tpu as pltpu
from jax.sharding import PartitionSpec as P

MESH = pl.DeviceIdType.MESH
SIDE = 4
STEPS = (1, -1)
OFFSETS = (0, -1, 1, 2)


def exchange_kernel(
    size,
    groups,
    factor,
    entries,
    x_hbm,
    oc_hbm,
    fc_hbm,
    vc_hbm,
    go_hbm,
    bases_hbm,
    fw_hbm,
    vw_hbm,
    ow_hbm,
    m1_hbm,
    m2_hbm,
    all_w,
    dirs,
    b_buf,
    scale_ref,
    n1_ref,
    n2_ref,
    fw_ref,
    vw_ref,
    ow_ref,
    m1_ref,
    m2_ref,
    x_buf,
    oc_buf,
    c_buf,
    acc,
    part,
    got,
    mine,
    sums,
    first_sem,
    load_sem,
    base_sem,
    w_send,
    w_recv,
    part_send,
    part_recv,
    dir_send,
    dir_recv,
    sum_send,
    sum_recv,
):
    me = lax.axis_index("fs")
    mt = lax.axis_index("tp")
    z = lax.div(me, SIDE)
    x = lax.rem(me, SIDE)
    tiles = load_sem.shape[1]
    tokens = x_buf.shape[0]
    rows_t = tokens // tiles
    rank_rows = m1_ref.shape[1]
    own = fw_ref.shape[0]
    half_rows = own // 2

    firsts = [
        pltpu.make_async_copy(src, dst, first_sem.at[i])
        for i, (src, dst) in enumerate(
            (
                (fw_hbm, fw_ref),
                (vw_hbm, vw_ref),
                (ow_hbm, ow_ref),
                (m1_hbm, m1_ref),
                (m2_hbm, m2_ref),
            )
        )
    ]
    for copy in firsts[:3]:
        copy.start()
    base_copies = [
        pltpu.make_async_copy(bases_hbm.at[k], b_buf.at[k], base_sem.at[k]) for k in range(3)
    ]

    def load(which, src, dst, tile):
        at = pl.ds(pl.multiple_of(tile * rows_t, rows_t), rows_t)
        return pltpu.make_async_copy(src.at[at, :], dst.at[at, :], load_sem.at[which, tile])

    streams = (
        (x_hbm, x_buf),
        (fc_hbm, c_buf.at[0]),
        (vc_hbm, c_buf.at[1]),
        (oc_hbm, oc_buf),
        (go_hbm, c_buf.at[2]),
    )
    base_copies[0].start()
    for tile in range(tiles):
        for which in (0, 1):
            load(which, *streams[which], tile).start()
    base_copies[1].start()
    for tile in range(tiles):
        load(2, *streams[2], tile).start()
    base_copies[2].start()
    for tile in range(tiles):
        for which in (3, 4):
            load(which, *streams[which], tile).start()
    for copy in firsts[3:]:
        copy.start()

    barrier = pltpu.get_barrier_semaphore()
    for j in range(1, size):
        pl.semaphore_signal(
            barrier, inc=1, device_id=(lax.rem(me + j, size), mt), device_id_type=MESH
        )
    for j in range(1, groups):
        pl.semaphore_signal(
            barrier, inc=1, device_id=(me, lax.rem(mt + j, groups)), device_id_type=MESH
        )
    for copy in firsts[:3]:
        copy.wait()
    all_w[me, 0] = fw_ref[...].astype(jnp.bfloat16)
    all_w[me, 1] = vw_ref[...].astype(jnp.bfloat16)
    all_w[me, 2, :, :own] = ow_ref[:own, :].astype(jnp.bfloat16)
    all_w[me, 2, :, own:] = ow_ref[own:, :].astype(jnp.bfloat16)

    def node(h, a, b):
        dz, dx = (b, a) if h == 0 else (a, b)
        return lax.rem(z + dz + SIDE, SIDE) * SIDE + lax.rem(x + dx + SIDE, SIDE)

    def w_copy(h, s, slot, owner, quarter, dest):
        start, count = h * half_rows, half_rows
        if quarter is not None:
            count = half_rows // 2
            start = start + quarter * count
        view = all_w.at[owner, :, pl.ds(start, count), :]
        return pltpu.make_async_remote_copy(
            src_ref=view,
            dst_ref=view,
            send_sem=w_send.at[h, s, slot],
            recv_sem=w_recv.at[h, s, slot],
            device_id=(dest, mt),
            device_id_type=MESH,
        )

    def near(h, s):
        return w_copy(h, s, 0, me, None, node(h, STEPS[s], 0))

    def near_on(h, s):
        return w_copy(h, s, 1, node(h, -STEPS[s], 0), s, node(h, STEPS[s], 0))

    def far(h, i, s):
        return w_copy(h, s, 2 + i, node(h, OFFSETS[i], 0), None, node(h, 0, STEPS[s]))

    def far_on(h, i, s):
        return w_copy(h, s, 6 + i, node(h, OFFSETS[i], -STEPS[s]), s, node(h, 0, STEPS[s]))

    def stage_0():
        for h in range(2):
            for s in range(2):
                near(h, s).start()
        for h in range(2):
            for s in range(2):
                far(h, 0, s).start()

    def stage_1():
        for h in range(2):
            for s in range(2):
                near(h, s).wait_recv()
        for h in range(2):
            for s in range(2):
                near_on(h, s).start()
        for i in (1, 2):
            for h in range(2):
                for s in range(2):
                    far(h, i, s).start()

    def stage_2():
        for h in range(2):
            for s in range(2):
                far(h, 0, s).wait_recv()
                far_on(h, 0, s).start()

    def stage_3():
        for h in range(2):
            for s in range(2):
                near_on(h, s).wait_recv()
        for h in range(2):
            for s in range(2):
                far(h, 3, s).start()

    def stage_on(i):
        for h in range(2):
            for s in range(2):
                far(h, i, s).wait_recv()
                far_on(h, i, s).start()

    def stage_last():
        for i in range(4):
            for h in range(2):
                for s in range(2):
                    far_on(h, i, s).wait_recv()

    def part_copy(k, j):
        owner = lax.rem(me + j, size)
        at = pl.ds(pl.multiple_of(owner * rank_rows, rank_rows), rank_rows)
        return pltpu.make_async_remote_copy(
            src_ref=part.at[k, at, :],
            dst_ref=got.at[k, j - 1],
            send_sem=part_send.at[k, j - 1],
            recv_sem=part_recv.at[k, j - 1],
            device_id=(owner, mt),
            device_id_type=MESH,
        )

    own_rows = pl.ds(pl.multiple_of(me * rank_rows, rank_rows), rank_rows)

    def dir_copy(k, j):
        return pltpu.make_async_remote_copy(
            src_ref=mine.at[k],
            dst_ref=dirs.at[k, own_rows, :],
            send_sem=dir_send.at[k, j - 1],
            recv_sem=dir_recv.at[k, j - 1],
            device_id=(lax.rem(me + j, size), mt),
            device_id_type=MESH,
        )

    def combine(k):
        projected = acc[k, own_rows, :] * factor
        for j in range(1, size):
            part_copy(k, j).wait_recv()
            projected = projected + got[k, j - 1].astype(jnp.float32)
        one = 0.9 * m1_ref[k] + 0.1 * projected
        two = 0.9 * m2_ref[k] + 0.1 * projected * projected
        n1_ref[k] = one
        n2_ref[k] = two
        rounded = (one / (jnp.sqrt(two) + 1e-08)).astype(jnp.bfloat16)
        mine[k] = rounded
        dirs[k, own_rows, :] = rounded
        for j in range(1, size):
            dir_copy(k, j).start()

    def compute(k, low, high):
        left_which, right_which = ((0, 1), (0, 2), (3, 4))[k]
        source = x_buf if k < 2 else oc_buf
        if low == 0:
            base_copies[k].wait()
            acc[k] = jnp.zeros(acc.shape[1:], acc.dtype)

        def tile_body(tile, carry):
            at = pl.ds(pl.multiple_of(tile * rows_t, rows_t), rows_t)
            if k != 1:
                load(left_which, *streams[left_which], tile).wait()
            reduced = jnp.dot(
                source[at, :], b_buf[k], preferred_element_type=jnp.float32
            ).astype(jnp.bfloat16)
            load(right_which, *streams[right_which], tile).wait()
            acc[k] += lax.dot_general(
                reduced,
                c_buf[k, at, :],
                (((0,), (0,)), ((), ())),
                preferred_element_type=jnp.float32,
            )
            return carry

        lax.fori_loop(low, high, tile_body, 0)

    def send_parts(k):
        part[k] = (acc[k] * factor).astype(jnp.bfloat16)
        for j in range(1, size):
            part_copy(k, j).start()

    with jax.named_scope("barrier"):
        pl.semaphore_wait(barrier, size - 1 + groups - 1)
    stage_0()
    with jax.named_scope("compute0"):
        compute(0, 0, tiles)
        send_parts(0)
    with jax.named_scope("compute1"):
        compute(1, 0, tiles)
        send_parts(1)
    with jax.named_scope("compute2a"):
        compute(2, 0, tiles // 2)
    with jax.named_scope("combine0"):
        for copy in firsts[3:]:
            copy.wait()
        combine(0)
    with jax.named_scope("compute2b"):
        compute(2, tiles // 2, tiles)
        send_parts(2)
    with jax.named_scope("stage1"):
        stage_1()
    with jax.named_scope("combine1"):
        combine(1)
    with jax.named_scope("combine2"):
        combine(2)
    with jax.named_scope("stage2"):
        stage_2()
    with jax.named_scope("stage3"):
        stage_3()
    with jax.named_scope("stage4"):
        stage_on(1)
        stage_on(2)

    row = lax.broadcasted_iota(jnp.int32, scale_ref.shape, 0)
    tile_sum = jnp.zeros(scale_ref.shape, jnp.float32)
    with jax.named_scope("dirs"):
        for k in range(3):
            for j in range(1, size):
                dir_copy(k, j).wait_recv()
            values = dirs[k].astype(jnp.float32)
            tile_sum = tile_sum + jnp.where(row == k, jnp.sum(values * values), 0.0)
        sums[0] = tile_sum

    def sum_copy(j):
        return pltpu.make_async_remote_copy(
            src_ref=sums.at[0],
            dst_ref=sums.at[j],
            send_sem=sum_send.at[j],
            recv_sem=sum_recv.at[j],
            device_id=(me, lax.rem(mt + j, groups)),
            device_id_type=MESH,
        )

    for j in range(1, groups):
        sum_copy(j).start()
    with jax.named_scope("stage5"):
        stage_on(3)
    with jax.named_scope("sums"):
        total = tile_sum
        for j in range(1, groups):
            sum_copy(j).wait_recv()
            total = total + sums[j]
        scale_ref[...] = lax.rsqrt(total / entries + 1.0)
    with jax.named_scope("stage6"):
        stage_last()

    with jax.named_scope("drain"):
        for h in range(2):
            for s in range(2):
                near(h, s).wait_send()
                near_on(h, s).wait_send()
                for i in range(4):
                    far(h, i, s).wait_send()
                    far_on(h, i, s).wait_send()
        for k in range(3):
            for j in range(1, size):
                part_copy(k, j).wait_send()
                dir_copy(k, j).wait_send()
        for j in range(1, groups):
            sum_copy(j).wait_send()


def exchange(size, groups, x, oc, fc, vc, go, bases, fw, vw, ow, m1, m2):
    tokens, width = x.shape
    rank = bases.shape[2]
    rows, columns = fw.shape
    rank_rows = m1.shape[1]
    tiles = 4
    bf16, f32 = jnp.bfloat16, jnp.float32
    vmem = pl.BlockSpec(memory_space=pltpu.VMEM)
    dma = pltpu.SemaphoreType.DMA
    kernel = functools.partial(
        exchange_kernel,
        size,
        groups,
        float(tokens * size) ** (-0.5),
        float(rank * columns * groups),
    )
    return pl.pallas_call(
        kernel,
        out_shape=(
            pltpu.VMEM((size, 3, rows, columns), bf16),
            pltpu.VMEM((3, rank, columns), bf16),
            pltpu.VMEM(bases.shape, bf16),
            pltpu.VMEM((8, 128), f32),
            pltpu.VMEM(m1.shape, f32),
            pltpu.VMEM(m2.shape, f32),
            pltpu.VMEM(fw.shape, f32),
            pltpu.VMEM(vw.shape, f32),
            pltpu.VMEM(ow.shape, f32),
        ),
        in_specs=[pl.BlockSpec(memory_space=pltpu.HBM)] * 11,
        out_specs=(vmem,) * 9,
        scratch_shapes=[
            pltpu.VMEM(m1.shape, f32),
            pltpu.VMEM(m2.shape, f32),
            pltpu.VMEM(x.shape, bf16),
            pltpu.VMEM(oc.shape, bf16),
            pltpu.VMEM((3, tokens, columns), bf16),
            pltpu.VMEM((3, rank, columns), f32),
            pltpu.VMEM((3, rank, columns), bf16),
            pltpu.VMEM((3, size - 1, rank_rows, columns), bf16),
            pltpu.VMEM((3, rank_rows, columns), bf16),
            pltpu.VMEM((groups, 8, 128), f32),
            dma((5,)),
            dma((5, tiles)),
            dma((3,)),
            dma((2, 2, 10)),
            dma((2, 2, 10)),
            dma((3, size - 1)),
            dma((3, size - 1)),
            dma((3, size - 1)),
            dma((3, size - 1)),
            dma((groups,)),
            dma((groups,)),
        ],
        compiler_params=pltpu.CompilerParams(
            collective_id=0, has_side_effects=True, vmem_limit_bytes=40 * 1024 * 1024
        ),
    )(x, oc, fc, vc, go, bases, fw, vw, ow, m1, m2)


def finish_kernel(
    scale_ref,
    dirs_ref,
    all_w,
    bases_ref,
    fw_ref,
    vw_ref,
    ow_ref,
    n1_ref,
    n2_ref,
    new_f,
    new_v,
    new_o,
    copy_f,
    copy_v,
    copy_o,
    n1_out,
    n2_out,
    step_f,
    step_v,
    step_o,
    cf_buf,
    cv_buf,
    co_buf,
    down_buf,
    across_buf,
    tile_sem,
    own_sem,
):
    tiles = tile_sem.shape[1]
    rows = cf_buf.shape[0] // tiles
    own = fw_ref.shape[0]
    owners = rows // own
    copies = []

    def put(src, dst, sem):
        copy = pltpu.make_async_copy(src, dst, sem)
        copy.start()
        copies.append(copy)

    put(n1_ref, n1_out, own_sem.at[6])
    put(n2_ref, n2_out, own_sem.at[7])

    def down(at, k):
        step = jnp.dot(bases_ref[k, at, :], dirs_ref[k], preferred_element_type=jnp.float32)
        return step * scale_ref[k : k + 1, 0:1]

    def across(at):
        step = lax.dot_general(
            dirs_ref[2],
            bases_ref[2, at, :],
            (((0,), (1,)), ((), ())),
            preferred_element_type=jnp.float32,
        )
        return step * scale_ref[2:3, 0:1]

    for tile in range(tiles):
        at = pl.ds(tile * rows, rows)
        owned = pl.ds(tile * owners, owners)
        for k, buf, out in ((0, cf_buf, copy_f), (1, cv_buf, copy_v)):
            old = all_w[owned, k].reshape(rows, cf_buf.shape[1])
            value = old.astype(jnp.float32) - 0.01 * down(at, k)
            buf[at, :] = value.astype(jnp.bfloat16)
            put(buf.at[at, :], out.at[at, :], tile_sem.at[k, tile])
        step = across(at)
        for i in range(owners):
            lanes = pl.ds(tile * rows + i * own, own)
            for j in range(2):
                old = all_w[tile * owners + i, 2, :, j * own : (j + 1) * own]
                value = old.astype(jnp.float32) - 0.01 * step[
                    j * own : (j + 1) * own, i * own : (i + 1) * own
                ]
                co_buf[pl.ds(j * own, own), lanes] = value.astype(jnp.bfloat16)
        put(co_buf.at[:, at], copy_o.at[:, at], tile_sem.at[2, tile])

    me = pl.ds(pl.multiple_of(lax.axis_index("fs") * own, own), own)
    for k, weight, new, out in ((0, fw_ref, new_f, step_f), (1, vw_ref, new_v, step_v)):
        step = down(me, k)
        down_buf[2 * k] = step
        put(down_buf.at[2 * k], out, own_sem.at[2 * k])
        down_buf[2 * k + 1] = weight[...] - 0.01 * step
        put(down_buf.at[2 * k + 1], new, own_sem.at[2 * k + 1])
    step = across(me)
    across_buf[0] = step
    put(across_buf.at[0], step_o, own_sem.at[4])
    across_buf[1] = ow_ref[...] - 0.01 * step
    put(across_buf.at[1], new_o, own_sem.at[5])

    for copy in copies:
        copy.wait()


def finish(all_w, dirs, bases, scales, one, two, fw, vw, ow):
    tiles = 4
    size, _, rows, columns = all_w.shape
    depth = size * rows
    rank = bases.shape[2]
    bf16, f32 = jnp.bfloat16, jnp.float32
    dma = pltpu.SemaphoreType.DMA
    tall = jax.ShapeDtypeStruct((depth, columns), bf16)
    wide = jax.ShapeDtypeStruct((columns, depth), bf16)
    down = jax.ShapeDtypeStruct((rows, columns), f32)
    across = jax.ShapeDtypeStruct((columns, rows), f32)
    small = jax.ShapeDtypeStruct(one.shape, f32)
    return pl.pallas_call(
        finish_kernel,
        out_shape=(down, down, across, tall, tall, wide, small, small, down, down, across),
        in_specs=[pl.BlockSpec(memory_space=pltpu.VMEM)] * 9,
        out_specs=(pl.BlockSpec(memory_space=pltpu.HBM),) * 11,
        scratch_shapes=[
            pltpu.VMEM(tall.shape, bf16),
            pltpu.VMEM(tall.shape, bf16),
            pltpu.VMEM(wide.shape, bf16),
            pltpu.VMEM((4,) + down.shape, f32),
            pltpu.VMEM((2,) + across.shape, f32),
            dma((3, tiles)),
            dma((8,)),
        ],
        compiler_params=pltpu.CompilerParams(vmem_limit_bytes=24 * 1024 * 1024),
        cost_estimate=pl.CostEstimate(
            flops=6 * depth * rank * columns, bytes_accessed=8 * depth * columns, transcendentals=0
        ),
    )(scales, dirs, all_w, bases, fw, vw, ow, one, two)


def on_device(
    normed_input,
    forget_cot,
    value_cot,
    gated_output,
    output_cot,
    forget_weight,
    value_weight,
    out_weight,
    bases,
    first_moment,
    second_moment,
):
    size, groups = lax.axis_size("fs"), lax.axis_size("tp")
    held = exchange(
        size,
        groups,
        normed_input,
        output_cot,
        forget_cot,
        value_cot,
        gated_output,
        bases,
        forget_weight,
        value_weight,
        out_weight,
        first_moment.transpose(1, 0, 2),
        second_moment.transpose(1, 0, 2),
    )
    outs = finish(*held)
    return (
        *outs[:6],
        outs[6].transpose(1, 0, 2),
        outs[7].transpose(1, 0, 2),
        *outs[8:],
    )


def solution(mesh):
    placed = (
        P("fs", None),
        P("fs", "tp"),
        P("fs", "tp"),
        P("fs", "tp"),
        P("fs", None),
        P("fs", "tp"),
        P("fs", "tp"),
        P("tp", "fs"),
        P(),
        P("fs", None, "tp"),
        P("fs", None, "tp"),
    )
    return jax.shard_map(
        on_device,
        mesh=mesh,
        in_specs=placed,
        out_specs=(
            P("fs", "tp"),
            P("fs", "tp"),
            P("tp", "fs"),
            P(None, "tp"),
            P(None, "tp"),
            P("tp", None),
            P("fs", None, "tp"),
            P("fs", None, "tp"),
            P("fs", "tp"),
            P("fs", "tp"),
            P("tp", "fs"),
        ),
        check_vma=False,
    )
```

time: 120 us -> 57.1 us (0.48)
  Pallas kernels: 118 us -> 46.2 us
  local copies, waits for them, and re-layouts: 0 us -> 9.86 us
    pallas_call x2, Pallas kernels: 118 us -> 46.2 us  [the longest x1 43.6 us: exchange(): pl.pallas_call(kernel, out_shape=(pltpu.VMEM((size, 3, rows, columns), bf...]
    unnamed x0 -> x18, local copies, waits for them, and re-layouts: none -> 9.86 us
where the time goes in v1:
time: 57.1 us; the launch traced here: 56.7 us
  Pallas kernels  46.2 us (81%)
  local copies, waits for them, and re-layouts  9.86 us (17%)
  between operations  0.67 us (1%)
    pallas_call x1, Pallas kernels, exchange(): pl.pallas_call(kernel, out_shape=(pltpu.VMEM((size, 3, rows, columns), bf...  43.6 us
    unnamed x18, local copies, waits for them, and re-layouts  9.86 us
    pallas_call x1, Pallas kernels, finish(): pl.pallas_call(finish_kernel, out_shape=(down, down, across, tall, tall,...  2.54 us

profile of v1, /device:TPU:0, one launch (start us, length us, event | category | flops | bytes accessed | tf_op | source)
XLA Modules:
  0.0 56.7 jit_solution(7075088486497711810)
XLA Ops:
  0.6 0.0 copy-start
  0.7 1.9 %copy-done = bf16[3,2048,256]{2,1,0:T(8,128)(2,1)S(1)} copy-done((bf16[3,2048,256]{2,1,0:T(8,128)(2,1)S(1)}, bf16[3,2048,256]{2,1,0:T(8,128)(2,1)}, u32[]{:S(2)}) %copy-start) | copy-done | bytes 3145752
  2.5 0.0 copy-start.1
  2.5 1.2 %copy-done.1 = bf16[2048,256]{1,0:T(8,128)(2,1)S(1)} copy-done((bf16[2048,256]{1,0:T(8,128)(2,1)S(1)}, bf16[2048,256]{1,0:T(8,128)(2,1)}, u32[]{:S(2)}) %copy-start.1) | copy-done | bytes 1048600
  3.8 0.0 copy-start.2
  3.8 1.2 %copy-done.2 = bf16[2048,256]{1,0:T(8,128)(2,1)S(1)} copy-done((bf16[2048,256]{1,0:T(8,128)(2,1)S(1)}, bf16[2048,256]{1,0:T(8,128)(2,1)}, u32[]{:S(2)}) %copy-start.2) | copy-done | bytes 1048600
  5.0 0.0 copy-start.3
  5.0 1.2 %copy-done.3 = bf16[2048,256]{1,0:T(8,128)(2,1)S(1)} copy-done((bf16[2048,256]{1,0:T(8,128)(2,1)S(1)}, bf16[2048,256]{1,0:T(8,128)(2,1)}, u32[]{:S(2)}) %copy-start.3) | copy-done | bytes 1048600
  6.2 0.0 copy-start.4
  6.2 0.9 %copy-done.4 = f32[128,256]{1,0:T(8,128)S(1)} copy-done((f32[128,256]{1,0:T(8,128)S(1)}, f32[128,256]{1,0:T(8,128)}, u32[]{:S(2)}) %copy-start.4) | copy-done | bytes 131096
  7.1 0.0 copy-start.5
  7.1 0.9 %copy-done.5 = f32[128,256]{1,0:T(8,128)S(1)} copy-done((f32[128,256]{1,0:T(8,128)S(1)}, f32[128,256]{1,0:T(8,128)}, u32[]{:S(2)}) %copy-start.5) | copy-done | bytes 131096
  8.0 0.0 copy-start.6
  8.0 0.9 %copy-done.6 = f32[256,128]{1,0:T(8,128)S(1)} copy-done((f32[256,128]{1,0:T(8,128)S(1)}, f32[256,128]{1,0:T(8,128)}, u32[]{:S(2)}) %copy-start.6) | copy-done | bytes 131096
  8.9 0.0 copy-start.7
  8.9 0.8 %copy-done.7 = f32[16,3,256]{2,0,1:T(8,128)S(1)} copy-done((f32[16,3,256]{2,0,1:T(8,128)S(1)}, f32[16,3,256]{2,0,1:T(8,128)}, u32[]{:S(2)}) %copy-start.7) | copy-done | bytes 49176
  9.7 0.0 copy-start.8
  9.7 0.8 %copy-done.8 = f32[16,3,256]{2,0,1:T(8,128)S(1)} copy-done((f32[16,3,256]{2,0,1:T(8,128)S(1)}, f32[16,3,256]{2,0,1:T(8,128)}, u32[]{:S(2)}) %copy-start.8) | copy-done | bytes 49176
  10.5 43.6 %shard_map.194 = (bf16[16,3,128,256]{3,2,1,0:T(8,128)(2,1)S(1)}, bf16[3,256,256]{2,1,0:T(8,128)(2,1)S(1)}, bf16[3,2048,256]{2,1,0:T(8,128)(2,1)S(1)}, f32[8,128]...) custom-call(bf16[2048,2048]{1,0:T(8,128)(2,1)} %x_hbm.1, ...), custom_call_target="tpu_custom_call" | custom-call | tf_op jit(solution)/shard_map/pallas_call | solution.py:376
  54.2 2.5 %shard_map.195 = (f32[128,256]{1,0:T(8,128)}, f32[128,256]{1,0:T(8,128)}, f32[256,128]{1,0:T(8,128)}, bf16[2048,256]{1,0:T(8,128)(2,1)}, bf16[2048,256]{1,0:T(8,...) custom-call(f32[8,128]{1,0:T(8,128)S(1)} %get-tuple-element.31.scale, ...), custom_call_target="tpu_custom_call" | custom-call | flops 805306368 | bytes 4194304 | tf_op jit(solution)/shard_map/pallas_call | solution.py:524
Async XLA Ops:
  0.6 1.9 %copy-start = (bf16[3,2048,256]{2,1,0:T(8,128)(2,1)S(1)}, bf16[3,2048,256]{2,1,0:T(8,128)(2,1)}, u32[]{:S(2)}) copy-start(bf16[3,2048,256]{2,1,0:T(8,128)(2,1)} %bases_hbm.1) | copy-start | bytes 9437188
  2.5 1.2 %copy-start.1 = (bf16[2048,256]{1,0:T(8,128)(2,1)S(1)}, bf16[2048,256]{1,0:T(8,128)(2,1)}, u32[]{:S(2)}) copy-start(bf16[2048,256]{1,0:T(8,128)(2,1)} %fc_hbm.1) | copy-start | bytes 3145732
  3.8 1.2 %copy-start.2 = (bf16[2048,256]{1,0:T(8,128)(2,1)S(1)}, bf16[2048,256]{1,0:T(8,128)(2,1)}, u32[]{:S(2)}) copy-start(bf16[2048,256]{1,0:T(8,128)(2,1)} %vc_hbm.1) | copy-start | bytes 3145732
  5.0 1.2 %copy-start.3 = (bf16[2048,256]{1,0:T(8,128)(2,1)S(1)}, bf16[2048,256]{1,0:T(8,128)(2,1)}, u32[]{:S(2)}) copy-start(bf16[2048,256]{1,0:T(8,128)(2,1)} %go_hbm.1) | copy-start | bytes 3145732
  6.2 0.9 %copy-start.4 = (f32[128,256]{1,0:T(8,128)S(1)}, f32[128,256]{1,0:T(8,128)}, u32[]{:S(2)}) copy-start(f32[128,256]{1,0:T(8,128)} %fw_hbm.1) | copy-start | bytes 393220
  7.1 0.9 %copy-start.5 = (f32[128,256]{1,0:T(8,128)S(1)}, f32[128,256]{1,0:T(8,128)}, u32[]{:S(2)}) copy-start(f32[128,256]{1,0:T(8,128)} %vw_hbm.1) | copy-start | bytes 393220
  8.0 0.9 %copy-start.6 = (f32[256,128]{1,0:T(8,128)S(1)}, f32[256,128]{1,0:T(8,128)}, u32[]{:S(2)}) copy-start(f32[256,128]{1,0:T(8,128)} %ow_hbm.1) | copy-start | bytes 393220
  8.9 0.8 %copy-start.7 = (f32[16,3,256]{2,0,1:T(8,128)S(1)}, f32[16,3,256]{2,0,1:T(8,128)}, u32[]{:S(2)}) copy-start(f32[16,3,256]{2,0,1:T(8,128)} %param.20) | copy-start | bytes 147460
  9.7 0.8 %copy-start.8 = (f32[16,3,256]{2,0,1:T(8,128)S(1)}, f32[16,3,256]{2,0,1:T(8,128)}, u32[]{:S(2)}) copy-start(f32[16,3,256]{2,0,1:T(8,128)} %param.21) | copy-start | bytes 147460

commit v2 on v1

--- a/solution.py
+++ b/solution.py
@@ -43,6 +43,7 @@
     x_buf,
     oc_buf,
     c_buf,
+    red,
     acc,
     part,
     got,
@@ -50,7 +51,10 @@
     sums,
     first_sem,
     load_sem,
+    cot_sem,
     base_sem,
+    pair_send,
+    pair_recv,
     w_send,
     w_recv,
     part_send,
@@ -64,9 +68,12 @@
     mt = lax.axis_index("tp")
     z = lax.div(me, SIDE)
     x = lax.rem(me, SIDE)
+    core = lax.rem(mt, 2)
+    partner = mt + 1 - 2 * core
     tiles = load_sem.shape[1]
-    tokens = x_buf.shape[0]
-    rows_t = tokens // tiles
+    tokens = c_buf.shape[1]
+    rows_t = x_buf.shape[0] // tiles
+    first_row = core * x_buf.shape[0]
     rank_rows = m1_ref.shape[1]
     own = fw_ref.shape[0]
     half_rows = own // 2
@@ -89,30 +96,22 @@
         pltpu.make_async_copy(bases_hbm.at[k], b_buf.at[k], base_sem.at[k]) for k in range(3)
     ]
 
+    def tile_rows(tile):
+        return pl.ds(pl.multiple_of(first_row + tile * rows_t, rows_t), rows_t)
+
     def load(which, src, dst, tile):
-        at = pl.ds(pl.multiple_of(tile * rows_t, rows_t), rows_t)
-        return pltpu.make_async_copy(src.at[at, :], dst.at[at, :], load_sem.at[which, tile])
-
-    streams = (
-        (x_hbm, x_buf),
-        (fc_hbm, c_buf.at[0]),
-        (vc_hbm, c_buf.at[1]),
-        (oc_hbm, oc_buf),
-        (go_hbm, c_buf.at[2]),
-    )
+        held = pl.ds(tile * rows_t, rows_t)
+        return pltpu.make_async_copy(
+            src.at[tile_rows(tile), :], dst.at[held, :], load_sem.at[which, tile]
+        )
+
+    def load_all(k):
+        return pltpu.make_async_copy((fc_hbm, vc_hbm, go_hbm)[k], c_buf.at[k], cot_sem.at[k])
+
+    streams = ((x_hbm, x_buf), (oc_hbm, oc_buf))
     base_copies[0].start()
-    for tile in range(tiles):
-        for which in (0, 1):
-            load(which, *streams[which], tile).start()
     base_copies[1].start()
-    for tile in range(tiles):
-        load(2, *streams[2], tile).start()
-    base_copies[2].start()
-    for tile in range(tiles):
-        for which in (3, 4):
-            load(which, *streams[which], tile).start()
-    for copy in firsts[3:]:
-        copy.start()
+    load(0, *streams[0], 0).start()
 
     barrier = pltpu.get_barrier_semaphore()
     for j in range(1, size):
@@ -125,6 +124,15 @@
         )
     for copy in firsts[:3]:
         copy.wait()
+    for tile in range(1, tiles):
+        load(0, *streams[0], tile).start()
+    base_copies[2].start()
+    for tile in range(tiles):
+        load(1, *streams[1], tile).start()
+    for k in range(3):
+        load_all(k).start()
+    for copy in firsts[3:]:
+        copy.start()
     all_w[me, 0] = fw_ref[...].astype(jnp.bfloat16)
     all_w[me, 1] = vw_ref[...].astype(jnp.bfloat16)
     all_w[me, 2, :, :own] = ow_ref[:own, :].astype(jnp.bfloat16)
@@ -176,10 +184,11 @@
         for h in range(2):
             for s in range(2):
                 near_on(h, s).start()
-        for i in (1, 2):
-            for h in range(2):
-                for s in range(2):
-                    far(h, i, s).start()
+
+    def stage_far(i):
+        for h in range(2):
+            for s in range(2):
+                far(h, i, s).start()
 
     def stage_2():
         for h in range(2):
@@ -191,9 +200,7 @@
         for h in range(2):
             for s in range(2):
                 near_on(h, s).wait_recv()
-        for h in range(2):
-            for s in range(2):
-                far(h, 3, s).start()
+        stage_far(3)
 
     def stage_on(i):
         for h in range(2):
@@ -246,33 +253,65 @@
         for j in range(1, size):
             dir_copy(k, j).start()
 
-    def compute(k, low, high):
-        left_which, right_which = ((0, 1), (0, 2), (3, 4))[k]
-        source = x_buf if k < 2 else oc_buf
-        if low == 0:
-            base_copies[k].wait()
-            acc[k] = jnp.zeros(acc.shape[1:], acc.dtype)
-
-        def tile_body(tile, carry):
-            at = pl.ds(pl.multiple_of(tile * rows_t, rows_t), rows_t)
-            if k != 1:
-                load(left_which, *streams[left_which], tile).wait()
-            reduced = jnp.dot(
-                source[at, :], b_buf[k], preferred_element_type=jnp.float32
-            ).astype(jnp.bfloat16)
-            load(right_which, *streams[right_which], tile).wait()
-            acc[k] += lax.dot_general(
-                reduced,
-                c_buf[k, at, :],
-                (((0,), (0,)), ((), ())),
-                preferred_element_type=jnp.float32,
-            )
-            return carry
-
-        lax.fori_loop(low, high, tile_body, 0)
+    def pair_copy(k, tile):
+        view = red.at[k, tile_rows(tile), :]
+        return pltpu.make_async_remote_copy(
+            src_ref=view,
+            dst_ref=view,
+            send_sem=pair_send.at[k, tile],
+            recv_sem=pair_recv.at[k, tile],
+            device_id=(me, partner),
+            device_id_type=MESH,
+        )
+
+    def reduce_pair(tile):
+        load(0, *streams[0], tile).wait()
+        rows = x_buf[pl.ds(tile * rows_t, rows_t), :]
+        first = jnp.dot(rows, b_buf[0], preferred_element_type=jnp.float32)
+        second = jnp.dot(rows, b_buf[1], preferred_element_type=jnp.float32)
+        red[0, tile_rows(tile), :] = first.astype(jnp.bfloat16)
+        red[1, tile_rows(tile), :] = second.astype(jnp.bfloat16)
+        for k in range(2):
+            pair_copy(k, tile).start()
+
+    def reduce_last(tile):
+        load(1, *streams[1], tile).wait()
+        half = rows_t // 2
+        upper, lower = pl.ds(tile * rows_t, half), pl.ds(tile * rows_t + half, half)
+        first = jnp.dot(oc_buf[upper, :], b_buf[2], preferred_element_type=jnp.float32)
+        second = jnp.dot(oc_buf[lower, :], b_buf[2], preferred_element_type=jnp.float32)
+        both = jnp.concatenate([first, second], axis=0)
+        red[2, tile_rows(tile), :] = both.astype(jnp.bfloat16)
+        pair_copy(2, tile).start()
+
+    def fold(left, right):
+        return lax.dot_general(
+            left, right, (((0,), (0,)), ((), ())), preferred_element_type=jnp.float32
+        )
+
+    def project_pair():
+        for k in range(2):
+            load_all(k).wait()
+            for tile in range(tiles):
+                pair_copy(k, tile).wait_recv()
+        first = fold(red[0], c_buf[0])
+        second = fold(red[1], c_buf[1])
+        acc[0] = first
+        acc[1] = second
+        part[0] = (first * factor).astype(jnp.bfloat16)
+        part[1] = (second * factor).astype(jnp.bfloat16)
+
+    def project_last():
+        load_all(2).wait()
+        for tile in range(tiles):
+            pair_copy(2, tile).wait_recv()
+        half = tokens // 2
+        total = fold(red[2, :half, :], c_buf[2, :half, :])
+        total = total + fold(red[2, half:, :], c_buf[2, half:, :])
+        acc[2] = total
+        part[2] = (total * factor).astype(jnp.bfloat16)
 
     def send_parts(k):
-        part[k] = (acc[k] * factor).astype(jnp.bfloat16)
         for j in range(1, size):
             part_copy(k, j).start()
 
@@ -280,33 +319,38 @@
         pl.semaphore_wait(barrier, size - 1 + groups - 1)
     stage_0()
     with jax.named_scope("compute0"):
-        compute(0, 0, tiles)
+        for k in range(2):
+            base_copies[k].wait()
+        for tile in range(tiles):
+            reduce_pair(tile)
+    with jax.named_scope("compute2"):
+        base_copies[2].wait()
+        for tile in range(tiles):
+            reduce_last(tile)
+    stage_1()
+    with jax.named_scope("project0"):
+        project_pair()
         send_parts(0)
-    with jax.named_scope("compute1"):
-        compute(1, 0, tiles)
         send_parts(1)
-    with jax.named_scope("compute2a"):
-        compute(2, 0, tiles // 2)
+    with jax.named_scope("project2"):
+        project_last()
+        send_parts(2)
+    stage_far(1)
+    for copy in firsts[3:]:
+        copy.wait()
     with jax.named_scope("combine0"):
-        for copy in firsts[3:]:
-            copy.wait()
         combine(0)
-    with jax.named_scope("compute2b"):
-        compute(2, tiles // 2, tiles)
-        send_parts(2)
-    with jax.named_scope("stage1"):
-        stage_1()
     with jax.named_scope("combine1"):
         combine(1)
     with jax.named_scope("combine2"):
         combine(2)
     with jax.named_scope("stage2"):
+        stage_far(2)
         stage_2()
     with jax.named_scope("stage3"):
         stage_3()
     with jax.named_scope("stage4"):
         stage_on(1)
-        stage_on(2)
 
     row = lax.broadcasted_iota(jnp.int32, scale_ref.shape, 0)
     tile_sum = jnp.zeros(scale_ref.shape, jnp.float32)
@@ -331,6 +375,7 @@
     for j in range(1, groups):
         sum_copy(j).start()
     with jax.named_scope("stage5"):
+        stage_on(2)
         stage_on(3)
     with jax.named_scope("sums"):
         total = tile_sum
@@ -353,6 +398,8 @@
             for j in range(1, size):
                 part_copy(k, j).wait_send()
                 dir_copy(k, j).wait_send()
+            for tile in range(tiles):
+                pair_copy(k, tile).wait_send()
         for j in range(1, groups):
             sum_copy(j).wait_send()
 
@@ -362,7 +409,7 @@
     rank = bases.shape[2]
     rows, columns = fw.shape
     rank_rows = m1.shape[1]
-    tiles = 4
+    tiles = 2
     bf16, f32 = jnp.bfloat16, jnp.float32
     vmem = pl.BlockSpec(memory_space=pltpu.VMEM)
     dma = pltpu.SemaphoreType.DMA
@@ -391,17 +438,21 @@
         scratch_shapes=[
             pltpu.VMEM(m1.shape, f32),
             pltpu.VMEM(m2.shape, f32),
-            pltpu.VMEM(x.shape, bf16),
-            pltpu.VMEM(oc.shape, bf16),
+            pltpu.VMEM((tokens // 2, width), bf16),
+            pltpu.VMEM((tokens // 2, width), bf16),
             pltpu.VMEM((3, tokens, columns), bf16),
+            pltpu.VMEM((3, tokens, rank), bf16),
             pltpu.VMEM((3, rank, columns), f32),
             pltpu.VMEM((3, rank, columns), bf16),
             pltpu.VMEM((3, size - 1, rank_rows, columns), bf16),
             pltpu.VMEM((3, rank_rows, columns), bf16),
             pltpu.VMEM((groups, 8, 128), f32),
             dma((5,)),
-            dma((5, tiles)),
+            dma((2, tiles)),
             dma((3,)),
+            dma((3,)),
+            dma((3, tiles)),
+            dma((3, tiles)),
             dma((2, 2, 10)),
             dma((2, 2, 10)),
             dma((3, size - 1)),
@@ -412,7 +463,7 @@
             dma((groups,)),
         ],
         compiler_params=pltpu.CompilerParams(
-            collective_id=0, has_side_effects=True, vmem_limit_bytes=40 * 1024 * 1024
+            collective_id=0, has_side_effects=True, vmem_limit_bytes=52 * 1024 * 1024
         ),
     )(x, oc, fc, vc, go, bases, fw, vw, ow, m1, m2)
 

time: 57.1 us -> 41.7 us (0.73)
  local copies, waits for them, and re-layouts: 9.86 us -> 0 us
  Pallas kernels: 46.2 us -> 41 us
    unnamed x18 -> x0, local copies, waits for them, and re-layouts: 9.86 us -> none
    pallas_call x1, Pallas kernels: 43.6 us -> 38.4 us  [exchange(): pl.pallas_call(kernel, out_shape=(pltpu.VMEM((size, 3, rows, columns), bf...]
where the time goes in v2:
time: 41.7 us; the launch traced here: 41.6 us
  Pallas kernels  41 us (98%)
  between operations  0.66 us (2%)
    pallas_call x1, Pallas kernels, exchange(): pl.pallas_call(kernel, out_shape=(pltpu.VMEM((size, 3, rows, columns), bf...  38.4 us
    pallas_call x1, Pallas kernels, finish(): pl.pallas_call(finish_kernel, out_shape=(down, down, across, tall, tall,...  2.54 us

profile of v2, /device:TPU:0, one launch (start us, length us, event | category | flops | bytes accessed | tf_op | source)
XLA Modules:
  0.0 41.6 jit_solution(17437708515134407942)
XLA Ops:
  0.6 38.4 %shard_map.194 = (bf16[16,3,128,256]{3,2,1,0:T(8,128)(2,1)S(1)}, bf16[3,256,256]{2,1,0:T(8,128)(2,1)S(1)}, bf16[3,2048,256]{2,1,0:T(8,128)(2,1)S(1)}, f32[8,128]...) custom-call(bf16[2048,2048]{1,0:T(8,128)(2,1)} %x_hbm.1, ...), custom_call_target="tpu_custom_call" | custom-call | tf_op jit(solution)/shard_map/pallas_call | solution.py:423
  39.1 2.5 %shard_map.195 = (f32[128,256]{1,0:T(8,128)}, f32[128,256]{1,0:T(8,128)}, f32[256,128]{1,0:T(8,128)}, bf16[2048,256]{1,0:T(8,128)(2,1)}, bf16[2048,256]{1,0:T(8,...) custom-call(f32[8,128]{1,0:T(8,128)S(1)} %get-tuple-element.31.scale, ...), custom_call_target="tpu_custom_call" | custom-call | flops 805306368 | bytes 4194304 | tf_op jit(solution)/shard_map/pallas_call | solution.py:575

commit v3 on v2

--- a/solution.py
+++ b/solution.py
@@ -47,21 +47,20 @@
     acc,
     part,
     got,
-    mine,
+    held,
+    mid,
+    last,
     sums,
+    totals,
     first_sem,
     load_sem,
     cot_sem,
     base_sem,
-    pair_send,
     pair_recv,
-    w_send,
+    send_sem,
     w_recv,
-    part_send,
     part_recv,
-    dir_send,
     dir_recv,
-    sum_send,
     sum_recv,
 ):
     me = lax.axis_index("fs")
@@ -75,6 +74,7 @@
     rows_t = x_buf.shape[0] // tiles
     first_row = core * x_buf.shape[0]
     rank_rows = m1_ref.shape[1]
+    columns = m1_ref.shape[2]
     own = fw_ref.shape[0]
     half_rows = own // 2
 
@@ -142,7 +142,7 @@
         dz, dx = (b, a) if h == 0 else (a, b)
         return lax.rem(z + dz + SIDE, SIDE) * SIDE + lax.rem(x + dx + SIDE, SIDE)
 
-    def w_copy(h, s, slot, owner, quarter, dest):
+    def w_copy(h, slot, owner, quarter, dest):
         start, count = h * half_rows, half_rows
         if quarter is not None:
             count = half_rows // 2
@@ -151,118 +151,173 @@
         return pltpu.make_async_remote_copy(
             src_ref=view,
             dst_ref=view,
-            send_sem=w_send.at[h, s, slot],
-            recv_sem=w_recv.at[h, s, slot],
+            send_sem=send_sem.at[0],
+            recv_sem=w_recv.at[slot],
             device_id=(dest, mt),
             device_id_type=MESH,
         )
 
     def near(h, s):
-        return w_copy(h, s, 0, me, None, node(h, STEPS[s], 0))
+        return w_copy(h, 0, me, None, node(h, STEPS[s], 0))
 
     def near_on(h, s):
-        return w_copy(h, s, 1, node(h, -STEPS[s], 0), s, node(h, STEPS[s], 0))
+        return w_copy(h, 1, node(h, -STEPS[s], 0), s, node(h, STEPS[s], 0))
 
     def far(h, i, s):
-        return w_copy(h, s, 2 + i, node(h, OFFSETS[i], 0), None, node(h, 0, STEPS[s]))
+        return w_copy(h, 2 + i, node(h, OFFSETS[i], 0), None, node(h, 0, STEPS[s]))
 
     def far_on(h, i, s):
-        return w_copy(h, s, 6 + i, node(h, OFFSETS[i], -STEPS[s]), s, node(h, 0, STEPS[s]))
-
-    def stage_0():
+        return w_copy(h, 6, node(h, OFFSETS[i], -STEPS[s]), s, node(h, 0, STEPS[s]))
+
+    def all_of(view, send, recv, to=None):
+        return pltpu.make_async_remote_copy(
+            src_ref=view,
+            dst_ref=view,
+            send_sem=send_sem.at[send],
+            recv_sem=recv,
+            device_id=(node(0, 1, 0), mt) if to is None else to,
+            device_id_type=MESH,
+        )
+
+    def w_arrived(slot):
+        count = (2, 1, 2, 2, 2, 2, 4)[slot]
+        all_of(all_w.at[pl.ds(0, count)], 0, w_recv.at[slot]).wait_recv()
+
+    def each(start):
         for h in range(2):
             for s in range(2):
-                near(h, s).start()
+                start(h, s).start()
+
+    def stage_0():
+        each(near)
+        stage_far(0)
+
+    def stage_1():
+        w_arrived(0)
+        each(near_on)
+
+    def stage_far(i):
+        each(lambda h, s: far(h, i, s))
+
+    def stage_on(i):
+        w_arrived(2 + i)
+        each(lambda h, s: far_on(h, i, s))
+
+    def stage_3():
+        w_arrived(1)
+        stage_far(3)
+
+    half_cols = columns // 2
+
+    def cut(h):
+        return pl.ds(h * half_cols, half_cols)
+
+    def line(h, second, j):
+        first_axis = (h == 0) != second
+        return (
+            z * SIDE + lax.rem(x + j, SIDE) if first_axis else lax.rem(z + j, SIDE) * SIDE + x
+        )
+
+    def blocks(ref, k, h, j):
+        if h == 0:
+            return ref.at[k, :, lax.rem(x + j, SIDE), :, cut(h)]
+        return ref.at[k, lax.rem(z + j, SIDE), :, :, cut(h)]
+
+    def move(src, dst, send, recv, dest):
+        return pltpu.make_async_remote_copy(
+            src_ref=src,
+            dst_ref=dst,
+            send_sem=send_sem.at[send],
+            recv_sem=recv,
+            device_id=(dest, mt),
+            device_id_type=MESH,
+        )
+
+    def part_first(k, h, j):
+        return move(
+            blocks(part, k, h, j), got.at[k, h, j - 1], 1, part_recv.at[0, k // 2], line(h, False, j)
+        )
+
+    def part_second(k, h, j):
+        place = lax.rem((z if h == 0 else x) + j, SIDE)
+        return move(
+            mid.at[k, h, place], last.at[k, h, j - 1], 2, part_recv.at[1, k // 2], line(h, True, j)
+        )
+
+    def dir_first(k, h, j):
+        view = dirs.at[k, z, x, :, cut(h)]
+        return move(view, view, 3, dir_recv.at[0], line(h, False, j))
+
+    def dir_second(k, h, j):
+        view = dirs.at[k, z, :, :, cut(h)] if h == 0 else dirs.at[k, :, x, :, cut(h)]
+        return move(view, view, 4, dir_recv.at[1], line(h, True, j))
+
+    def group_of(ref, ks):
+        return ref.at[pl.ds(ks[0], len(ks))]
+
+    ALL = [(h, j) for h in range(2) for j in range(1, SIDE)]
+
+    def send_parts(k):
+        for h, j in ALL:
+            part_first(k, h, j).start()
+
+    def pass_parts(ks):
+        all_of(group_of(got, ks), 1, part_recv.at[0, ks[0] // 2]).wait_recv()
+        for k in ks:
+            for h in range(2):
+                own_part = acc[k, :, x, :, cut(h)] if h == 0 else acc[k, z, :, :, cut(h)]
+                total = own_part * factor
+                for j in range(1, SIDE):
+                    total = total + got[k, h, j - 1].astype(jnp.float32)
+                held[k, h] = total
+                mid[k, h] = total.astype(jnp.bfloat16)
+                for j in range(1, SIDE):
+                    part_second(k, h, j).start()
+
+    lane = lax.broadcasted_iota(jnp.int32, sums.shape[1:], 1)
+
+    def combine(ks):
+        all_of(group_of(last, ks), 2, part_recv.at[1, ks[0] // 2]).wait_recv()
+        return sum(update(k) for k in ks)
+
+    def update(k):
+        square = jnp.zeros((rank_rows, half_cols), jnp.float32)
         for h in range(2):
-            for s in range(2):
-                far(h, 0, s).start()
-
-    def stage_1():
-        for h in range(2):
-            for s in range(2):
-                near(h, s).wait_recv()
-        for h in range(2):
-            for s in range(2):
-                near_on(h, s).start()
-
-    def stage_far(i):
-        for h in range(2):
-            for s in range(2):
-                far(h, i, s).start()
-
-    def stage_2():
-        for h in range(2):
-            for s in range(2):
-                far(h, 0, s).wait_recv()
-                far_on(h, 0, s).start()
-
-    def stage_3():
-        for h in range(2):
-            for s in range(2):
-                near_on(h, s).wait_recv()
-        stage_far(3)
-
-    def stage_on(i):
-        for h in range(2):
-            for s in range(2):
-                far(h, i, s).wait_recv()
-                far_on(h, i, s).start()
-
-    def stage_last():
-        for i in range(4):
-            for h in range(2):
-                for s in range(2):
-                    far_on(h, i, s).wait_recv()
-
-    def part_copy(k, j):
-        owner = lax.rem(me + j, size)
-        at = pl.ds(pl.multiple_of(owner * rank_rows, rank_rows), rank_rows)
-        return pltpu.make_async_remote_copy(
-            src_ref=part.at[k, at, :],
-            dst_ref=got.at[k, j - 1],
-            send_sem=part_send.at[k, j - 1],
-            recv_sem=part_recv.at[k, j - 1],
-            device_id=(owner, mt),
-            device_id_type=MESH,
-        )
-
-    own_rows = pl.ds(pl.multiple_of(me * rank_rows, rank_rows), rank_rows)
-
-    def dir_copy(k, j):
-        return pltpu.make_async_remote_copy(
-            src_ref=mine.at[k],
-            dst_ref=dirs.at[k, own_rows, :],
-            send_sem=dir_send.at[k, j - 1],
-            recv_sem=dir_recv.at[k, j - 1],
-            device_id=(lax.rem(me + j, size), mt),
-            device_id_type=MESH,
-        )
-
-    def combine(k):
-        projected = acc[k, own_rows, :] * factor
-        for j in range(1, size):
-            part_copy(k, j).wait_recv()
-            projected = projected + got[k, j - 1].astype(jnp.float32)
-        one = 0.9 * m1_ref[k] + 0.1 * projected
-        two = 0.9 * m2_ref[k] + 0.1 * projected * projected
-        n1_ref[k] = one
-        n2_ref[k] = two
-        rounded = (one / (jnp.sqrt(two) + 1e-08)).astype(jnp.bfloat16)
-        mine[k] = rounded
-        dirs[k, own_rows, :] = rounded
-        for j in range(1, size):
-            dir_copy(k, j).start()
+            projected = held[k, h, z if h == 0 else x]
+            for j in range(1, SIDE):
+                projected = projected + last[k, h, j - 1].astype(jnp.float32)
+            one = 0.9 * m1_ref[k, :, cut(h)] + 0.1 * projected
+            two = 0.9 * m2_ref[k, :, cut(h)] + 0.1 * projected * projected
+            n1_ref[k, :, cut(h)] = one
+            n2_ref[k, :, cut(h)] = two
+            rounded = (one / (jnp.sqrt(two) + 1e-08)).astype(jnp.bfloat16)
+            dirs[k, z, x, :, cut(h)] = rounded
+            for j in range(1, SIDE):
+                dir_first(k, h, j).start()
+            value = rounded.astype(jnp.float32)
+            square = square + value * value
+        return jnp.where(lane == k, jnp.sum(square), 0.0)
+
+    def pass_dirs():
+        all_of(last, 3, dir_recv.at[0]).wait_recv()
+        for k in range(3):
+            for h, j in ALL:
+                dir_second(k, h, j).start()
 
     def pair_copy(k, tile):
         view = red.at[k, tile_rows(tile), :]
         return pltpu.make_async_remote_copy(
             src_ref=view,
             dst_ref=view,
-            send_sem=pair_send.at[k, tile],
-            recv_sem=pair_recv.at[k, tile],
+            send_sem=send_sem.at[5],
+            recv_sem=pair_recv.at[k // 2],
             device_id=(me, partner),
             device_id_type=MESH,
         )
+
+    def pair_half(ks, recv):
+        view = red.at[ks, pl.ds(0, tokens // 2), :]
+        return all_of(view, 5, recv, (me, partner))
 
     def reduce_pair(tile):
         load(0, *streams[0], tile).wait()
@@ -292,28 +347,23 @@
     def project_pair():
         for k in range(2):
             load_all(k).wait()
-            for tile in range(tiles):
-                pair_copy(k, tile).wait_recv()
+        pair_half(pl.ds(0, 2), pair_recv.at[0]).wait_recv()
+        shape = acc.shape[1:]
         first = fold(red[0], c_buf[0])
         second = fold(red[1], c_buf[1])
-        acc[0] = first
-        acc[1] = second
-        part[0] = (first * factor).astype(jnp.bfloat16)
-        part[1] = (second * factor).astype(jnp.bfloat16)
+        acc[0] = first.reshape(shape)
+        acc[1] = second.reshape(shape)
+        part[0] = (first * factor).astype(jnp.bfloat16).reshape(shape)
+        part[1] = (second * factor).astype(jnp.bfloat16).reshape(shape)
 
     def project_last():
         load_all(2).wait()
-        for tile in range(tiles):
-            pair_copy(2, tile).wait_recv()
+        pair_half(pl.ds(2, 1), pair_recv.at[1]).wait_recv()
         half = tokens // 2
         total = fold(red[2, :half, :], c_buf[2, :half, :])
         total = total + fold(red[2, half:, :], c_buf[2, half:, :])
-        acc[2] = total
-        part[2] = (total * factor).astype(jnp.bfloat16)
-
-    def send_parts(k):
-        for j in range(1, size):
-            part_copy(k, j).start()
+        acc[2] = total.reshape(acc.shape[1:])
+        part[2] = (total * factor).astype(jnp.bfloat16).reshape(acc.shape[1:])
 
     with jax.named_scope("barrier"):
         pl.semaphore_wait(barrier, size - 1 + groups - 1)
@@ -336,72 +386,85 @@
         project_last()
         send_parts(2)
     stage_far(1)
+    stage_on(0)
+    with jax.named_scope("pass0"):
+        pass_parts((0, 1))
+    with jax.named_scope("pass2"):
+        pass_parts((2,))
+    stage_far(2)
     for copy in firsts[3:]:
         copy.wait()
-    with jax.named_scope("combine0"):
-        combine(0)
-    with jax.named_scope("combine1"):
-        combine(1)
-    with jax.named_scope("combine2"):
-        combine(2)
-    with jax.named_scope("stage2"):
-        stage_far(2)
-        stage_2()
-    with jax.named_scope("stage3"):
-        stage_3()
-    with jax.named_scope("stage4"):
-        stage_on(1)
-
-    row = lax.broadcasted_iota(jnp.int32, scale_ref.shape, 0)
-    tile_sum = jnp.zeros(scale_ref.shape, jnp.float32)
-    with jax.named_scope("dirs"):
-        for k in range(3):
-            for j in range(1, size):
-                dir_copy(k, j).wait_recv()
-            values = dirs[k].astype(jnp.float32)
-            tile_sum = tile_sum + jnp.where(row == k, jnp.sum(values * values), 0.0)
-        sums[0] = tile_sum
+    def total_copy(j):
+        return pltpu.make_async_remote_copy(
+            src_ref=totals.at[0],
+            dst_ref=totals.at[j],
+            send_sem=send_sem.at[6],
+            recv_sem=sum_recv.at[1],
+            device_id=(lax.rem(me + j, size), mt),
+            device_id_type=MESH,
+        )
 
     def sum_copy(j):
         return pltpu.make_async_remote_copy(
             src_ref=sums.at[0],
             dst_ref=sums.at[j],
-            send_sem=sum_send.at[j],
-            recv_sem=sum_recv.at[j],
+            send_sem=send_sem.at[7],
+            recv_sem=sum_recv.at[0],
             device_id=(me, lax.rem(mt + j, groups)),
             device_id_type=MESH,
         )
 
+    def sums_arrived():
+        return all_of(sums.at[pl.ds(1, groups - 1)], 7, sum_recv.at[0])
+
+    def totals_arrived():
+        return all_of(totals.at[pl.ds(1, size - 1)], 6, sum_recv.at[1])
+
+    with jax.named_scope("combine0"):
+        own_sum = combine((0, 1))
+    with jax.named_scope("combine2"):
+        sums[0] = own_sum + combine((2,))
     for j in range(1, groups):
         sum_copy(j).start()
+    with jax.named_scope("stage2"):
+        stage_on(1)
+        stage_3()
+    with jax.named_scope("dirs1"):
+        pass_dirs()
+    with jax.named_scope("stage3"):
+        stage_on(2)
+    with jax.named_scope("sums"):
+        sums_arrived().wait_recv()
+        total = sums[0]
+        for j in range(1, groups):
+            total = total + sums[j]
+        totals[0] = total
+        for j in range(1, size):
+            total_copy(j).start()
+
+    with jax.named_scope("dirs2"):
+        all_of(got, 4, dir_recv.at[1]).wait_recv()
     with jax.named_scope("stage5"):
-        stage_on(2)
         stage_on(3)
-    with jax.named_scope("sums"):
-        total = tile_sum
-        for j in range(1, groups):
-            sum_copy(j).wait_recv()
-            total = total + sums[j]
-        scale_ref[...] = lax.rsqrt(total / entries + 1.0)
+    with jax.named_scope("totals"):
+        totals_arrived().wait_recv()
+        for j in range(1, size):
+            total = total + totals[j]
+        scale = lax.rsqrt(total / entries + 1.0)
+        for k in range(3):
+            scale_ref[k] = jnp.broadcast_to(scale[:, k : k + 1], scale_ref.shape[1:])
     with jax.named_scope("stage6"):
-        stage_last()
+        w_arrived(6)
 
     with jax.named_scope("drain"):
-        for h in range(2):
-            for s in range(2):
-                near(h, s).wait_send()
-                near_on(h, s).wait_send()
-                for i in range(4):
-                    far(h, i, s).wait_send()
-                    far_on(h, i, s).wait_send()
-        for k in range(3):
-            for j in range(1, size):
-                part_copy(k, j).wait_send()
-                dir_copy(k, j).wait_send()
-            for tile in range(tiles):
-                pair_copy(k, tile).wait_send()
-        for j in range(1, groups):
-            sum_copy(j).wait_send()
+        all_of(all_w.at[pl.ds(0, size - 1)], 0, w_recv.at[0]).wait_send()
+        all_of(got, 1, dir_recv.at[1]).wait_send()
+        all_of(last, 2, dir_recv.at[0]).wait_send()
+        all_of(last, 3, dir_recv.at[0]).wait_send()
+        all_of(got, 4, dir_recv.at[1]).wait_send()
+        pair_half(pl.ds(0, 3), pair_recv.at[0]).wait_send()
+        totals_arrived().wait_send()
+        sums_arrived().wait_send()
 
 
 def exchange(size, groups, x, oc, fc, vc, go, bases, fw, vw, ow, m1, m2):
@@ -424,9 +487,9 @@
         kernel,
         out_shape=(
             pltpu.VMEM((size, 3, rows, columns), bf16),
-            pltpu.VMEM((3, rank, columns), bf16),
+            pltpu.VMEM((3, SIDE, SIDE, rank_rows, columns), bf16),
             pltpu.VMEM(bases.shape, bf16),
-            pltpu.VMEM((8, 128), f32),
+            pltpu.VMEM((3, 8, 512), f32),
             pltpu.VMEM(m1.shape, f32),
             pltpu.VMEM(m2.shape, f32),
             pltpu.VMEM(fw.shape, f32),
@@ -442,25 +505,24 @@
             pltpu.VMEM((tokens // 2, width), bf16),
             pltpu.VMEM((3, tokens, columns), bf16),
             pltpu.VMEM((3, tokens, rank), bf16),
-            pltpu.VMEM((3, rank, columns), f32),
-            pltpu.VMEM((3, rank, columns), bf16),
-            pltpu.VMEM((3, size - 1, rank_rows, columns), bf16),
-            pltpu.VMEM((3, rank_rows, columns), bf16),
-            pltpu.VMEM((groups, 8, 128), f32),
+            pltpu.VMEM((3, SIDE, SIDE, rank_rows, columns), f32),
+            pltpu.VMEM((3, SIDE, SIDE, rank_rows, columns), bf16),
+            pltpu.VMEM((3, 2, SIDE - 1, SIDE, rank_rows, columns // 2), bf16),
+            pltpu.VMEM((3, 2, SIDE, rank_rows, columns // 2), f32),
+            pltpu.VMEM((3, 2, SIDE, rank_rows, columns // 2), bf16),
+            pltpu.VMEM((3, 2, SIDE - 1, rank_rows, columns // 2), bf16),
+            pltpu.VMEM((groups, 1, 128), f32),
+            pltpu.VMEM((size, 1, 128), f32),
             dma((5,)),
             dma((2, tiles)),
             dma((3,)),
             dma((3,)),
-            dma((3, tiles)),
-            dma((3, tiles)),
-            dma((2, 2, 10)),
-            dma((2, 2, 10)),
-            dma((3, size - 1)),
-            dma((3, size - 1)),
-            dma((3, size - 1)),
-            dma((3, size - 1)),
-            dma((groups,)),
-            dma((groups,)),
+            dma((2,)),
+            dma((8,)),
+            dma((7,)),
+            dma((2, 2)),
+            dma((2,)),
+            dma((2,)),
         ],
         compiler_params=pltpu.CompilerParams(
             collective_id=0, has_side_effects=True, vmem_limit_bytes=52 * 1024 * 1024
@@ -495,34 +557,34 @@
     down_buf,
     across_buf,
     tile_sem,
-    own_sem,
+    small_sem,
 ):
-    tiles = tile_sem.shape[1]
+    tiles = 4
     rows = cf_buf.shape[0] // tiles
     own = fw_ref.shape[0]
     owners = rows // own
-    copies = []
 
     def put(src, dst, sem):
-        copy = pltpu.make_async_copy(src, dst, sem)
-        copy.start()
-        copies.append(copy)
-
-    put(n1_ref, n1_out, own_sem.at[6])
-    put(n2_ref, n2_out, own_sem.at[7])
+        pltpu.make_async_copy(src, dst, sem).start()
+
+    put(n1_ref, n1_out, small_sem.at[0])
+    put(n2_ref, n2_out, small_sem.at[1])
+
+    def direction(k):
+        return dirs_ref[k].reshape(bases_ref.shape[2], down_buf.shape[2])
 
     def down(at, k):
-        step = jnp.dot(bases_ref[k, at, :], dirs_ref[k], preferred_element_type=jnp.float32)
-        return step * scale_ref[k : k + 1, 0:1]
+        step = jnp.dot(bases_ref[k, at, :], direction(k), preferred_element_type=jnp.float32)
+        return step * scale_ref[k, 0:1, : step.shape[1]]
 
     def across(at):
         step = lax.dot_general(
-            dirs_ref[2],
+            direction(2),
             bases_ref[2, at, :],
             (((0,), (1,)), ((), ())),
             preferred_element_type=jnp.float32,
         )
-        return step * scale_ref[2:3, 0:1]
+        return step * scale_ref[2, 0:1, : step.shape[1]]
 
     for tile in range(tiles):
         at = pl.ds(tile * rows, rows)
@@ -531,7 +593,7 @@
             old = all_w[owned, k].reshape(rows, cf_buf.shape[1])
             value = old.astype(jnp.float32) - 0.01 * down(at, k)
             buf[at, :] = value.astype(jnp.bfloat16)
-            put(buf.at[at, :], out.at[at, :], tile_sem.at[k, tile])
+            put(buf.at[at, :], out.at[at, :], tile_sem.at[k])
         step = across(at)
         for i in range(owners):
             lanes = pl.ds(tile * rows + i * own, own)
@@ -541,27 +603,30 @@
                     j * own : (j + 1) * own, i * own : (i + 1) * own
                 ]
                 co_buf[pl.ds(j * own, own), lanes] = value.astype(jnp.bfloat16)
-        put(co_buf.at[:, at], copy_o.at[:, at], tile_sem.at[2, tile])
+        put(co_buf.at[:, at], copy_o.at[:, at], tile_sem.at[2])
 
     me = pl.ds(pl.multiple_of(lax.axis_index("fs") * own, own), own)
     for k, weight, new, out in ((0, fw_ref, new_f, step_f), (1, vw_ref, new_v, step_v)):
         step = down(me, k)
         down_buf[2 * k] = step
-        put(down_buf.at[2 * k], out, own_sem.at[2 * k])
+        put(down_buf.at[2 * k], out, small_sem.at[2])
         down_buf[2 * k + 1] = weight[...] - 0.01 * step
-        put(down_buf.at[2 * k + 1], new, own_sem.at[2 * k + 1])
+        put(down_buf.at[2 * k + 1], new, small_sem.at[2])
     step = across(me)
     across_buf[0] = step
-    put(across_buf.at[0], step_o, own_sem.at[4])
+    put(across_buf.at[0], step_o, small_sem.at[3])
     across_buf[1] = ow_ref[...] - 0.01 * step
-    put(across_buf.at[1], new_o, own_sem.at[5])
-
-    for copy in copies:
-        copy.wait()
+    put(across_buf.at[1], new_o, small_sem.at[3])
+
+    for i, buf, out in ((0, cf_buf, copy_f), (1, cv_buf, copy_v), (2, co_buf, copy_o)):
+        pltpu.make_async_copy(buf, out, tile_sem.at[i]).wait()
+    pltpu.make_async_copy(n1_ref, n1_out, small_sem.at[0]).wait()
+    pltpu.make_async_copy(n2_ref, n2_out, small_sem.at[1]).wait()
+    pltpu.make_async_copy(down_buf, down_buf, small_sem.at[2]).wait()
+    pltpu.make_async_copy(across_buf, across_buf, small_sem.at[3]).wait()
 
 
 def finish(all_w, dirs, bases, scales, one, two, fw, vw, ow):
-    tiles = 4
     size, _, rows, columns = all_w.shape
     depth = size * rows
     rank = bases.shape[2]
@@ -583,8 +648,8 @@
             pltpu.VMEM(wide.shape, bf16),
             pltpu.VMEM((4,) + down.shape, f32),
             pltpu.VMEM((2,) + across.shape, f32),
-            dma((3, tiles)),
-            dma((8,)),
+            dma((3,)),
+            dma((4,)),
         ],
         compiler_params=pltpu.CompilerParams(vmem_limit_bytes=24 * 1024 * 1024),
         cost_estimate=pl.CostEstimate(

time: 41.7 us -> 37.4 us (0.90)
  Pallas kernels: 41 us -> 36.7 us
    pallas_call x1, Pallas kernels: 38.4 us -> 34.3 us  [exchange(): pl.pallas_call(kernel, out_shape=(pltpu.VMEM((size, 3, rows, columns), bf...]
where the time goes in v3:
time: 37.4 us; the launch traced here: 37.3 us
  Pallas kernels  36.7 us (98%)
  between operations  0.66 us (2%)
    pallas_call x1, Pallas kernels, exchange(): pl.pallas_call(kernel, out_shape=(pltpu.VMEM((size, 3, rows, columns), bf...  34.3 us
    pallas_call x1, Pallas kernels, finish(): pl.pallas_call(finish_kernel, out_shape=(down, down, across, tall, tall,...  2.32 us

profile of v3, /device:TPU:0, one launch (start us, length us, event | category | flops | bytes accessed | tf_op | source)
XLA Modules:
  0.0 37.3 jit_solution(11349337149300007241)
XLA Ops:
  0.6 34.3 %shard_map.194 = (bf16[16,3,128,256]{3,2,1,0:T(8,128)(2,1)S(1)}, bf16[3,4,4,16,256]{4,3,2,1,0:T(8,128)(2,1)S(1)}, bf16[3,2048,256]{2,1,0:T(8,128)(2,1)S(1)}, f32...) custom-call(bf16[2048,2048]{1,0:T(8,128)(2,1)} %x_hbm.1, ...), custom_call_target="tpu_custom_call" | custom-call | tf_op jit(solution)/shard_map/pallas_call | solution.py:486
  35.0 2.3 %shard_map.195 = (f32[128,256]{1,0:T(8,128)}, f32[128,256]{1,0:T(8,128)}, f32[256,128]{1,0:T(8,128)}, bf16[2048,256]{1,0:T(8,128)(2,1)}, bf16[2048,256]{1,0:T(8,...) custom-call(f32[3,8,512]{2,1,0:T(8,128)S(1)} %get-tuple-element.31.s, ...), custom_call_target="tpu_custom_call" | custom-call | flops 805306368 | bytes 4194304 | tf_op jit(solution)/shard_map/pallas_call | solution.py:640

commit v4 on v3

--- a/solution.py
+++ b/solution.py
@@ -62,6 +62,9 @@
     part_recv,
     dir_recv,
     sum_recv,
+    near_sem,
+    across_sem,
+    plane_sem,
 ):
     me = lax.axis_index("fs")
     mt = lax.axis_index("tp")
@@ -113,26 +116,19 @@
     base_copies[1].start()
     load(0, *streams[0], 0).start()
 
+    def ahead(dz, dx):
+        return lax.rem(z + dz, SIDE) * SIDE + lax.rem(x + dx, SIDE)
+
+    def along_y(step):
+        return lax.rem(mt + 2 * step, groups)
+
     barrier = pltpu.get_barrier_semaphore()
-    for j in range(1, size):
-        pl.semaphore_signal(
-            barrier, inc=1, device_id=(lax.rem(me + j, size), mt), device_id_type=MESH
-        )
-    for j in range(1, groups):
-        pl.semaphore_signal(
-            barrier, inc=1, device_id=(me, lax.rem(mt + j, groups)), device_id_type=MESH
-        )
+    around = [(ahead(0, 1), mt), (ahead(0, 3), mt), (ahead(1, 0), mt), (ahead(3, 0), mt)]
+    around += [(me, along_y(1)), (me, along_y(3)), (me, partner)]
+    for place in around:
+        pl.semaphore_signal(barrier, inc=1, device_id=place, device_id_type=MESH)
     for copy in firsts[:3]:
         copy.wait()
-    for tile in range(1, tiles):
-        load(0, *streams[0], tile).start()
-    base_copies[2].start()
-    for tile in range(tiles):
-        load(1, *streams[1], tile).start()
-    for k in range(3):
-        load_all(k).start()
-    for copy in firsts[3:]:
-        copy.start()
     all_w[me, 0] = fw_ref[...].astype(jnp.bfloat16)
     all_w[me, 1] = vw_ref[...].astype(jnp.bfloat16)
     all_w[me, 2, :, :own] = ow_ref[:own, :].astype(jnp.bfloat16)
@@ -365,8 +361,20 @@
         acc[2] = total.reshape(acc.shape[1:])
         part[2] = (total * factor).astype(jnp.bfloat16).reshape(acc.shape[1:])
 
+    for tile in range(1, tiles):
+        load(0, *streams[0], tile).start()
+    base_copies[2].start()
+    for tile in range(tiles):
+        load(1, *streams[1], tile).start()
+    for k in range(3):
+        load_all(k).start()
+    for copy in firsts[3:]:
+        copy.start()
     with jax.named_scope("barrier"):
-        pl.semaphore_wait(barrier, size - 1 + groups - 1)
+        pl.semaphore_wait(barrier, len(around))
+    next_to = [around[0], around[2], around[4], around[5]]
+    for place in next_to:
+        pl.semaphore_signal(near_sem, inc=1, device_id=place, device_id_type=MESH)
     stage_0()
     with jax.named_scope("compute0"):
         for k in range(2):
@@ -380,6 +388,14 @@
     stage_1()
     with jax.named_scope("project0"):
         project_pair()
+        pl.semaphore_wait(near_sem, len(next_to))
+        pl.semaphore_signal(
+            across_sem, inc=1, device_id=(me, along_y(2)), device_id_type=MESH
+        )
+        for step in range(1, SIDE):
+            pl.semaphore_signal(
+                plane_sem, inc=1, device_id=(ahead(0, step), mt), device_id_type=MESH
+            )
         send_parts(0)
         send_parts(1)
     with jax.named_scope("project2"):
@@ -424,6 +440,7 @@
         own_sum = combine((0, 1))
     with jax.named_scope("combine2"):
         sums[0] = own_sum + combine((2,))
+    pl.semaphore_wait(across_sem, 1)
     for j in range(1, groups):
         sum_copy(j).start()
     with jax.named_scope("stage2"):
@@ -431,21 +448,22 @@
         stage_3()
     with jax.named_scope("dirs1"):
         pass_dirs()
-    with jax.named_scope("stage3"):
-        stage_on(2)
     with jax.named_scope("sums"):
         sums_arrived().wait_recv()
         total = sums[0]
         for j in range(1, groups):
             total = total + sums[j]
         totals[0] = total
+        pl.semaphore_wait(plane_sem, SIDE - 1)
         for j in range(1, size):
             total_copy(j).start()
 
+    with jax.named_scope("stage3"):
+        stage_on(2)
+    with jax.named_scope("stage5"):
+        stage_on(3)
     with jax.named_scope("dirs2"):
         all_of(got, 4, dir_recv.at[1]).wait_recv()
-    with jax.named_scope("stage5"):
-        stage_on(3)
     with jax.named_scope("totals"):
         totals_arrived().wait_recv()
         for j in range(1, size):
@@ -523,6 +541,9 @@
             dma((2, 2)),
             dma((2,)),
             dma((2,)),
+            pltpu.SemaphoreType.REGULAR,
+            pltpu.SemaphoreType.REGULAR,
+            pltpu.SemaphoreType.REGULAR,
         ],
         compiler_params=pltpu.CompilerParams(
             collective_id=0, has_side_effects=True, vmem_limit_bytes=52 * 1024 * 1024

time: 37.4 us -> 35.2 us (0.941)
  Pallas kernels: 36.7 us -> 34.4 us
    pallas_call x1, Pallas kernels: 34.3 us -> 32.1 us  [exchange(): pl.pallas_call(kernel, out_shape=(pltpu.VMEM((size, 3, rows, columns), bf...]
where the time goes in v4:
time: 35.2 us; the launch traced here: 35.1 us
  Pallas kernels  34.4 us (98%)
  between operations  0.66 us (2%)
    pallas_call x1, Pallas kernels, exchange(): pl.pallas_call(kernel, out_shape=(pltpu.VMEM((size, 3, rows, columns), bf...  32.1 us
    pallas_call x1, Pallas kernels, finish(): pl.pallas_call(finish_kernel, out_shape=(down, down, across, tall, tall,...  2.32 us

profile of v4, /device:TPU:0, one launch (start us, length us, event | category | flops | bytes accessed | tf_op | source)
XLA Modules:
  0.0 35.1 jit_solution(7456416741067914071)
XLA Ops:
  0.6 32.1 %shard_map.194 = (bf16[16,3,128,256]{3,2,1,0:T(8,128)(2,1)S(1)}, bf16[3,4,4,16,256]{4,3,2,1,0:T(8,128)(2,1)S(1)}, bf16[3,2048,256]{2,1,0:T(8,128)(2,1)S(1)}, f32...) custom-call(bf16[2048,2048]{1,0:T(8,128)(2,1)} %x_hbm.1, ...), custom_call_target="tpu_custom_call" | custom-call | tf_op jit(solution)/shard_map/pallas_call | solution.py:504
  32.8 2.3 %shard_map.195 = (f32[128,256]{1,0:T(8,128)}, f32[128,256]{1,0:T(8,128)}, f32[256,128]{1,0:T(8,128)}, bf16[2048,256]{1,0:T(8,128)(2,1)}, bf16[2048,256]{1,0:T(8,...) custom-call(f32[3,8,512]{2,1,0:T(8,128)S(1)} %get-tuple-element.31.s, ...), custom_call_target="tpu_custom_call" | custom-call | flops 805306368 | bytes 4194304 | tf_op jit(solution)/shard_map/pallas_call | solution.py:661

commit v5 on v4

--- a/solution.py
+++ b/solution.py
@@ -72,9 +72,9 @@
     x = lax.rem(me, SIDE)
     core = lax.rem(mt, 2)
     partner = mt + 1 - 2 * core
-    tiles = load_sem.shape[1]
     tokens = c_buf.shape[1]
-    rows_t = x_buf.shape[0] // tiles
+    quarter_rows = x_buf.shape[0] // 4
+    cuts = (((0, 1), (1, 2), (3, 1)), ((0, 2), (2, 2)))
     first_row = core * x_buf.shape[0]
     rank_rows = m1_ref.shape[1]
     columns = m1_ref.shape[2]
@@ -99,13 +99,20 @@
         pltpu.make_async_copy(bases_hbm.at[k], b_buf.at[k], base_sem.at[k]) for k in range(3)
     ]
 
-    def tile_rows(tile):
-        return pl.ds(pl.multiple_of(first_row + tile * rows_t, rows_t), rows_t)
+    def tile_rows(which, tile):
+        start, count = cuts[which][tile]
+        rows = count * quarter_rows
+        return pl.ds(pl.multiple_of(first_row + start * quarter_rows, quarter_rows), rows)
+
+    def held_rows(which, tile):
+        start, count = cuts[which][tile]
+        return pl.ds(start * quarter_rows, count * quarter_rows)
 
     def load(which, src, dst, tile):
-        held = pl.ds(tile * rows_t, rows_t)
         return pltpu.make_async_copy(
-            src.at[tile_rows(tile), :], dst.at[held, :], load_sem.at[which, tile]
+            src.at[tile_rows(which, tile), :],
+            dst.at[held_rows(which, tile), :],
+            load_sem.at[which, tile],
         )
 
     def load_all(k):
@@ -113,8 +120,8 @@
 
     streams = ((x_hbm, x_buf), (oc_hbm, oc_buf))
     base_copies[0].start()
+    load(0, *streams[0], 0).start()
     base_copies[1].start()
-    load(0, *streams[0], 0).start()
 
     def ahead(dz, dx):
         return lax.rem(z + dz, SIDE) * SIDE + lax.rem(x + dx, SIDE)
@@ -242,11 +249,11 @@
 
     def dir_first(k, h, j):
         view = dirs.at[k, z, x, :, cut(h)]
-        return move(view, view, 3, dir_recv.at[0], line(h, False, j))
+        return move(view, view, 3, dir_recv.at[k // 2], line(h, False, j))
 
     def dir_second(k, h, j):
         view = dirs.at[k, z, :, :, cut(h)] if h == 0 else dirs.at[k, :, x, :, cut(h)]
-        return move(view, view, 4, dir_recv.at[1], line(h, True, j))
+        return move(view, view, 4, dir_recv.at[2], line(h, True, j))
 
     def group_of(ref, ks):
         return ref.at[pl.ds(ks[0], len(ks))]
@@ -294,14 +301,14 @@
             square = square + value * value
         return jnp.where(lane == k, jnp.sum(square), 0.0)
 
-    def pass_dirs():
-        all_of(last, 3, dir_recv.at[0]).wait_recv()
-        for k in range(3):
+    def pass_dirs(ks):
+        all_of(group_of(last, ks), 3, dir_recv.at[ks[0] // 2]).wait_recv()
+        for k in ks:
             for h, j in ALL:
                 dir_second(k, h, j).start()
 
     def pair_copy(k, tile):
-        view = red.at[k, tile_rows(tile), :]
+        view = red.at[k, tile_rows(k // 2, tile), :]
         return pltpu.make_async_remote_copy(
             src_ref=view,
             dst_ref=view,
@@ -317,22 +324,25 @@
 
     def reduce_pair(tile):
         load(0, *streams[0], tile).wait()
-        rows = x_buf[pl.ds(tile * rows_t, rows_t), :]
+        rows = x_buf[held_rows(0, tile), :]
+        at = tile_rows(0, tile)
         first = jnp.dot(rows, b_buf[0], preferred_element_type=jnp.float32)
         second = jnp.dot(rows, b_buf[1], preferred_element_type=jnp.float32)
-        red[0, tile_rows(tile), :] = first.astype(jnp.bfloat16)
-        red[1, tile_rows(tile), :] = second.astype(jnp.bfloat16)
+        red[0, at, :] = first.astype(jnp.bfloat16)
+        red[1, at, :] = second.astype(jnp.bfloat16)
         for k in range(2):
             pair_copy(k, tile).start()
 
     def reduce_last(tile):
         load(1, *streams[1], tile).wait()
-        half = rows_t // 2
-        upper, lower = pl.ds(tile * rows_t, half), pl.ds(tile * rows_t + half, half)
+        start, count = cuts[1][tile]
+        half = count * quarter_rows // 2
+        upper = pl.ds(start * quarter_rows, half)
+        lower = pl.ds(start * quarter_rows + half, half)
         first = jnp.dot(oc_buf[upper, :], b_buf[2], preferred_element_type=jnp.float32)
         second = jnp.dot(oc_buf[lower, :], b_buf[2], preferred_element_type=jnp.float32)
         both = jnp.concatenate([first, second], axis=0)
-        red[2, tile_rows(tile), :] = both.astype(jnp.bfloat16)
+        red[2, tile_rows(1, tile), :] = both.astype(jnp.bfloat16)
         pair_copy(2, tile).start()
 
     def fold(left, right):
@@ -361,15 +371,8 @@
         acc[2] = total.reshape(acc.shape[1:])
         part[2] = (total * factor).astype(jnp.bfloat16).reshape(acc.shape[1:])
 
-    for tile in range(1, tiles):
+    for tile in range(1, len(cuts[0])):
         load(0, *streams[0], tile).start()
-    base_copies[2].start()
-    for tile in range(tiles):
-        load(1, *streams[1], tile).start()
-    for k in range(3):
-        load_all(k).start()
-    for copy in firsts[3:]:
-        copy.start()
     with jax.named_scope("barrier"):
         pl.semaphore_wait(barrier, len(around))
     next_to = [around[0], around[2], around[4], around[5]]
@@ -379,11 +382,20 @@
     with jax.named_scope("compute0"):
         for k in range(2):
             base_copies[k].wait()
-        for tile in range(tiles):
+        for tile in range(len(cuts[0])):
             reduce_pair(tile)
+            if tile == 0:
+                base_copies[2].start()
+                for later in range(len(cuts[1])):
+                    load(1, *streams[1], later).start()
+            elif tile == 1:
+                for k in range(3):
+                    load_all(k).start()
+                for copy in firsts[3:]:
+                    copy.start()
     with jax.named_scope("compute2"):
         base_copies[2].wait()
-        for tile in range(tiles):
+        for tile in range(len(cuts[1])):
             reduce_last(tile)
     stage_1()
     with jax.named_scope("project0"):
@@ -437,6 +449,7 @@
         return all_of(totals.at[pl.ds(1, size - 1)], 6, sum_recv.at[1])
 
     with jax.named_scope("combine0"):
+        stage_on(1)
         own_sum = combine((0, 1))
     with jax.named_scope("combine2"):
         sums[0] = own_sum + combine((2,))
@@ -444,10 +457,10 @@
     for j in range(1, groups):
         sum_copy(j).start()
     with jax.named_scope("stage2"):
-        stage_on(1)
         stage_3()
+        stage_on(2)
     with jax.named_scope("dirs1"):
-        pass_dirs()
+        pass_dirs((0, 1))
     with jax.named_scope("sums"):
         sums_arrived().wait_recv()
         total = sums[0]
@@ -458,12 +471,12 @@
         for j in range(1, size):
             total_copy(j).start()
 
-    with jax.named_scope("stage3"):
-        stage_on(2)
+    with jax.named_scope("dirs1b"):
+        pass_dirs((2,))
     with jax.named_scope("stage5"):
         stage_on(3)
     with jax.named_scope("dirs2"):
-        all_of(got, 4, dir_recv.at[1]).wait_recv()
+        all_of(got, 4, dir_recv.at[2]).wait_recv()
     with jax.named_scope("totals"):
         totals_arrived().wait_recv()
         for j in range(1, size):
@@ -476,10 +489,10 @@
 
     with jax.named_scope("drain"):
         all_of(all_w.at[pl.ds(0, size - 1)], 0, w_recv.at[0]).wait_send()
-        all_of(got, 1, dir_recv.at[1]).wait_send()
+        all_of(got, 1, dir_recv.at[2]).wait_send()
         all_of(last, 2, dir_recv.at[0]).wait_send()
         all_of(last, 3, dir_recv.at[0]).wait_send()
-        all_of(got, 4, dir_recv.at[1]).wait_send()
+        all_of(got, 4, dir_recv.at[2]).wait_send()
         pair_half(pl.ds(0, 3), pair_recv.at[0]).wait_send()
         totals_arrived().wait_send()
         sums_arrived().wait_send()
@@ -490,7 +503,6 @@
     rank = bases.shape[2]
     rows, columns = fw.shape
     rank_rows = m1.shape[1]
-    tiles = 2
     bf16, f32 = jnp.bfloat16, jnp.float32
     vmem = pl.BlockSpec(memory_space=pltpu.VMEM)
     dma = pltpu.SemaphoreType.DMA
@@ -532,14 +544,14 @@
             pltpu.VMEM((groups, 1, 128), f32),
             pltpu.VMEM((size, 1, 128), f32),
             dma((5,)),
-            dma((2, tiles)),
+            dma((2, 3)),
             dma((3,)),
             dma((3,)),
             dma((2,)),
             dma((8,)),
             dma((7,)),
             dma((2, 2)),
-            dma((2,)),
+            dma((3,)),
             dma((2,)),
             pltpu.SemaphoreType.REGULAR,
             pltpu.SemaphoreType.REGULAR,
@@ -607,6 +619,19 @@
         )
         return step * scale_ref[2, 0:1, : step.shape[1]]
 
+    me = pl.ds(pl.multiple_of(lax.axis_index("fs") * own, own), own)
+    for k, weight, new, out in ((0, fw_ref, new_f, step_f), (1, vw_ref, new_v, step_v)):
+        step = down(me, k)
+        down_buf[2 * k] = step
+        put(down_buf.at[2 * k], out, small_sem.at[2])
+        down_buf[2 * k + 1] = weight[...] - 0.01 * step
+        put(down_buf.at[2 * k + 1], new, small_sem.at[2])
+    step = across(me)
+    across_buf[0] = step
+    put(across_buf.at[0], step_o, small_sem.at[3])
+    across_buf[1] = ow_ref[...] - 0.01 * step
+    put(across_buf.at[1], new_o, small_sem.at[3])
+
     for tile in range(tiles):
         at = pl.ds(tile * rows, rows)
         owned = pl.ds(tile * owners, owners)
@@ -625,19 +650,6 @@
                 ]
                 co_buf[pl.ds(j * own, own), lanes] = value.astype(jnp.bfloat16)
         put(co_buf.at[:, at], copy_o.at[:, at], tile_sem.at[2])
-
-    me = pl.ds(pl.multiple_of(lax.axis_index("fs") * own, own), own)
-    for k, weight, new, out in ((0, fw_ref, new_f, step_f), (1, vw_ref, new_v, step_v)):
-        step = down(me, k)
-        down_buf[2 * k] = step
-        put(down_buf.at[2 * k], out, small_sem.at[2])
-        down_buf[2 * k + 1] = weight[...] - 0.01 * step
-        put(down_buf.at[2 * k + 1], new, small_sem.at[2])
-    step = across(me)
-    across_buf[0] = step
-    put(across_buf.at[0], step_o, small_sem.at[3])
-    across_buf[1] = ow_ref[...] - 0.01 * step
-    put(across_buf.at[1], new_o, small_sem.at[3])
 
     for i, buf, out in ((0, cf_buf, copy_f), (1, cv_buf, copy_v), (2, co_buf, copy_o)):
         pltpu.make_async_copy(buf, out, tile_sem.at[i]).wait()

time: 35.2 us -> 34.9 us (level)
  no operation moved by 1% of the time
where the time goes in v5:
time: 34.9 us; the launch traced here: 34.8 us
  Pallas kernels  34.1 us (98%)
  between operations  0.66 us (2%)
    pallas_call x1, Pallas kernels, exchange(): pl.pallas_call(kernel, out_shape=(pltpu.VMEM((size, 3, rows, columns), bf...  31.9 us
    pallas_call x1, Pallas kernels, finish(): pl.pallas_call(finish_kernel, out_shape=(down, down, across, tall, tall,...  2.21 us

profile of v5, /device:TPU:0, one launch (start us, length us, event | category | flops | bytes accessed | tf_op | source)
XLA Modules:
  0.0 34.8 jit_solution(3871994874479060110)
XLA Ops:
  0.6 31.9 %shard_map.194 = (bf16[16,3,128,256]{3,2,1,0:T(8,128)(2,1)S(1)}, bf16[3,4,4,16,256]{4,3,2,1,0:T(8,128)(2,1)S(1)}, bf16[3,2048,256]{2,1,0:T(8,128)(2,1)S(1)}, f32...) custom-call(bf16[2048,2048]{1,0:T(8,128)(2,1)} %x_hbm.1, ...), custom_call_target="tpu_custom_call" | custom-call | tf_op jit(solution)/shard_map/pallas_call | solution.py:516
  32.6 2.2 %shard_map.195 = (f32[128,256]{1,0:T(8,128)}, f32[128,256]{1,0:T(8,128)}, f32[256,128]{1,0:T(8,128)}, bf16[2048,256]{1,0:T(8,128)(2,1)}, bf16[2048,256]{1,0:T(8,...) custom-call(f32[3,8,512]{2,1,0:T(8,128)S(1)} %get-tuple-element.31.s, ...), custom_call_target="tpu_custom_call" | custom-call | flops 805306368 | bytes 4194304 | tf_op jit(solution)/shard_map/pallas_call | solution.py:673

commit v6 on v5

--- a/solution.py
+++ b/solution.py
@@ -64,7 +64,6 @@
     sum_recv,
     near_sem,
     across_sem,
-    plane_sem,
 ):
     me = lax.axis_index("fs")
     mt = lax.axis_index("tp")
@@ -404,10 +403,6 @@
         pl.semaphore_signal(
             across_sem, inc=1, device_id=(me, along_y(2)), device_id_type=MESH
         )
-        for step in range(1, SIDE):
-            pl.semaphore_signal(
-                plane_sem, inc=1, device_id=(ahead(0, step), mt), device_id_type=MESH
-            )
         send_parts(0)
         send_parts(1)
     with jax.named_scope("project2"):
@@ -416,6 +411,7 @@
     stage_far(1)
     stage_on(0)
     with jax.named_scope("pass0"):
+        pl.semaphore_wait(across_sem, 1)
         pass_parts((0, 1))
     with jax.named_scope("pass2"):
         pass_parts((2,))
@@ -428,7 +424,7 @@
             dst_ref=totals.at[j],
             send_sem=send_sem.at[6],
             recv_sem=sum_recv.at[1],
-            device_id=(lax.rem(me + j, size), mt),
+            device_id=(ahead(0, j), mt),
             device_id_type=MESH,
         )
 
@@ -438,48 +434,48 @@
             dst_ref=sums.at[j],
             send_sem=send_sem.at[7],
             recv_sem=sum_recv.at[0],
-            device_id=(me, lax.rem(mt + j, groups)),
+            device_id=(ahead(j // groups, 0), lax.rem(mt + j % groups, groups)),
             device_id_type=MESH,
         )
 
     def sums_arrived():
-        return all_of(sums.at[pl.ds(1, groups - 1)], 7, sum_recv.at[0])
+        return all_of(sums.at[pl.ds(1, SIDE * groups - 1)], 7, sum_recv.at[0])
 
     def totals_arrived():
-        return all_of(totals.at[pl.ds(1, size - 1)], 6, sum_recv.at[1])
+        return all_of(totals.at[pl.ds(1, SIDE - 1)], 6, sum_recv.at[1])
 
     with jax.named_scope("combine0"):
         stage_on(1)
         own_sum = combine((0, 1))
     with jax.named_scope("combine2"):
         sums[0] = own_sum + combine((2,))
-    pl.semaphore_wait(across_sem, 1)
-    for j in range(1, groups):
+    for j in range(1, SIDE * groups):
         sum_copy(j).start()
     with jax.named_scope("stage2"):
         stage_3()
         stage_on(2)
     with jax.named_scope("dirs1"):
         pass_dirs((0, 1))
+    with jax.named_scope("dirs1b"):
+        pass_dirs((2,))
+    with jax.named_scope("stage5n"):
+        pl.when(core == 1)(lambda: stage_on(3))
     with jax.named_scope("sums"):
         sums_arrived().wait_recv()
         total = sums[0]
-        for j in range(1, groups):
+        for j in range(1, SIDE * groups):
             total = total + sums[j]
         totals[0] = total
-        pl.semaphore_wait(plane_sem, SIDE - 1)
-        for j in range(1, size):
+        for j in range(1, SIDE):
             total_copy(j).start()
 
-    with jax.named_scope("dirs1b"):
-        pass_dirs((2,))
     with jax.named_scope("stage5"):
-        stage_on(3)
+        pl.when(core == 0)(lambda: stage_on(3))
     with jax.named_scope("dirs2"):
         all_of(got, 4, dir_recv.at[2]).wait_recv()
     with jax.named_scope("totals"):
         totals_arrived().wait_recv()
-        for j in range(1, size):
+        for j in range(1, SIDE):
             total = total + totals[j]
         scale = lax.rsqrt(total / entries + 1.0)
         for k in range(3):
@@ -541,8 +537,8 @@
             pltpu.VMEM((3, 2, SIDE, rank_rows, columns // 2), f32),
             pltpu.VMEM((3, 2, SIDE, rank_rows, columns // 2), bf16),
             pltpu.VMEM((3, 2, SIDE - 1, rank_rows, columns // 2), bf16),
-            pltpu.VMEM((groups, 1, 128), f32),
-            pltpu.VMEM((size, 1, 128), f32),
+            pltpu.VMEM((SIDE * groups, 1, 128), f32),
+            pltpu.VMEM((SIDE, 1, 128), f32),
             dma((5,)),
             dma((2, 3)),
             dma((3,)),
@@ -553,7 +549,6 @@
             dma((2, 2)),
             dma((3,)),
             dma((2,)),
-            pltpu.SemaphoreType.REGULAR,
             pltpu.SemaphoreType.REGULAR,
             pltpu.SemaphoreType.REGULAR,
         ],

time: 34.9 us -> 34.5 us (0.989)
  Pallas kernels: 34.1 us -> 33.6 us
    pallas_call x1, Pallas kernels: 31.9 us -> 31.4 us  [exchange(): pl.pallas_call(kernel, out_shape=(pltpu.VMEM((size, 3, rows, columns), bf...]
where the time goes in v6:
time: 34.5 us; the launch traced here: 34.3 us
  Pallas kernels  33.6 us (97%)
  between operations  0.66 us (2%)
    pallas_call x1, Pallas kernels, exchange(): pl.pallas_call(kernel, out_shape=(pltpu.VMEM((size, 3, rows, columns), bf...  31.4 us
    pallas_call x1, Pallas kernels, finish(): pl.pallas_call(finish_kernel, out_shape=(down, down, across, tall, tall,...  2.22 us

profile of v6, /device:TPU:0, one launch (start us, length us, event | category | flops | bytes accessed | tf_op | source)
XLA Modules:
  0.0 34.3 jit_solution(4713511239300326949)
XLA Ops:
  0.6 31.4 %shard_map.194 = (bf16[16,3,128,256]{3,2,1,0:T(8,128)(2,1)S(1)}, bf16[3,4,4,16,256]{4,3,2,1,0:T(8,128)(2,1)S(1)}, bf16[3,2048,256]{2,1,0:T(8,128)(2,1)S(1)}, f32...) custom-call(bf16[2048,2048]{1,0:T(8,128)(2,1)} %x_hbm.1, ...), custom_call_target="tpu_custom_call" | custom-call | tf_op jit(solution)/shard_map/pallas_call | solution.py:512
  32.1 2.2 %shard_map.195 = (f32[128,256]{1,0:T(8,128)}, f32[128,256]{1,0:T(8,128)}, f32[256,128]{1,0:T(8,128)}, bf16[2048,256]{1,0:T(8,128)(2,1)}, bf16[2048,256]{1,0:T(8,...) custom-call(f32[3,8,512]{2,1,0:T(8,128)S(1)} %get-tuple-element.31.s, ...), custom_call_target="tpu_custom_call" | custom-call | flops 805306368 | bytes 4194304 | tf_op jit(solution)/shard_map/pallas_call | solution.py:668

commit v7 on v6

--- a/solution.py
+++ b/solution.py
@@ -118,9 +118,9 @@
         return pltpu.make_async_copy((fc_hbm, vc_hbm, go_hbm)[k], c_buf.at[k], cot_sem.at[k])
 
     streams = ((x_hbm, x_buf), (oc_hbm, oc_buf))
-    base_copies[0].start()
-    load(0, *streams[0], 0).start()
-    base_copies[1].start()
+    base_copies[0].start(priority=1)
+    load(0, *streams[0], 0).start(priority=1)
+    base_copies[1].start(priority=1)
 
     def ahead(dz, dx):
         return lax.rem(z + dz, SIDE) * SIDE + lax.rem(x + dx, SIDE)
@@ -257,7 +257,8 @@
     def group_of(ref, ks):
         return ref.at[pl.ds(ks[0], len(ks))]
 
-    ALL = [(h, j) for h in range(2) for j in range(1, SIDE)]
+    FIRST = (2, 1, 3)
+    ALL = [(h, j) for j in FIRST for h in range(2)]
 
     def send_parts(k):
         for h, j in ALL:
@@ -273,7 +274,7 @@
                     total = total + got[k, h, j - 1].astype(jnp.float32)
                 held[k, h] = total
                 mid[k, h] = total.astype(jnp.bfloat16)
-                for j in range(1, SIDE):
+                for j in FIRST:
                     part_second(k, h, j).start()
 
     lane = lax.broadcasted_iota(jnp.int32, sums.shape[1:], 1)
@@ -294,7 +295,7 @@
             n2_ref[k, :, cut(h)] = two
             rounded = (one / (jnp.sqrt(two) + 1e-08)).astype(jnp.bfloat16)
             dirs[k, z, x, :, cut(h)] = rounded
-            for j in range(1, SIDE):
+            for j in FIRST:
                 dir_first(k, h, j).start()
             value = rounded.astype(jnp.float32)
             square = square + value * value
@@ -302,8 +303,8 @@
 
     def pass_dirs(ks):
         all_of(group_of(last, ks), 3, dir_recv.at[ks[0] // 2]).wait_recv()
-        for k in ks:
-            for h, j in ALL:
+        for h, j in ALL:
+            for k in ks:
                 dir_second(k, h, j).start()
 
     def pair_copy(k, tile):
@@ -371,7 +372,7 @@
         part[2] = (total * factor).astype(jnp.bfloat16).reshape(acc.shape[1:])
 
     for tile in range(1, len(cuts[0])):
-        load(0, *streams[0], tile).start()
+        load(0, *streams[0], tile).start(priority=1)
     with jax.named_scope("barrier"):
         pl.semaphore_wait(barrier, len(around))
     next_to = [around[0], around[2], around[4], around[5]]
@@ -449,8 +450,10 @@
         own_sum = combine((0, 1))
     with jax.named_scope("combine2"):
         sums[0] = own_sum + combine((2,))
-    for j in range(1, SIDE * groups):
-        sum_copy(j).start()
+    for dz in (2, 1, 3, 0):
+        for dt in (4, 5, 3, 2, 6, 7, 1, 0):
+            if dz + dt > 0:
+                sum_copy(dz * groups + dt).start()
     with jax.named_scope("stage2"):
         stage_3()
         stage_on(2)
@@ -466,7 +469,7 @@
         for j in range(1, SIDE * groups):
             total = total + sums[j]
         totals[0] = total
-        for j in range(1, SIDE):
+        for j in FIRST:
             total_copy(j).start()
 
     with jax.named_scope("stage5"):
@@ -587,7 +590,7 @@
     tile_sem,
     small_sem,
 ):
-    tiles = 4
+    tiles = 8
     rows = cf_buf.shape[0] // tiles
     own = fw_ref.shape[0]
     owners = rows // own

time: 34.5 us -> 34.7 us (level)
  no operation moved by 1% of the time
where the time goes in v7:
time: 34.7 us; the launch traced here: 34.6 us
  Pallas kernels  33.9 us (98%)
  between operations  0.66 us (2%)
    pallas_call x1, Pallas kernels, exchange(): pl.pallas_call(kernel, out_shape=(pltpu.VMEM((size, 3, rows, columns), bf...  31.7 us
    pallas_call x1, Pallas kernels, finish(): pl.pallas_call(finish_kernel, out_shape=(down, down, across, tall, tall,...  2.17 us

profile of v7, /device:TPU:0, one launch (start us, length us, event | category | flops | bytes accessed | tf_op | source)
XLA Modules:
  0.0 34.6 jit_solution(16926506465282990426)
XLA Ops:
  0.6 31.7 %shard_map.194 = (bf16[16,3,128,256]{3,2,1,0:T(8,128)(2,1)S(1)}, bf16[3,4,4,16,256]{4,3,2,1,0:T(8,128)(2,1)S(1)}, bf16[3,2048,256]{2,1,0:T(8,128)(2,1)S(1)}, f32...) custom-call(bf16[2048,2048]{1,0:T(8,128)(2,1)} %x_hbm.1, ...), custom_call_target="tpu_custom_call" | custom-call | tf_op jit(solution)/shard_map/pallas_call | solution.py:515
  32.4 2.2 %shard_map.195 = (f32[128,256]{1,0:T(8,128)}, f32[128,256]{1,0:T(8,128)}, f32[256,128]{1,0:T(8,128)}, bf16[2048,256]{1,0:T(8,128)(2,1)}, bf16[2048,256]{1,0:T(8,...) custom-call(f32[3,8,512]{2,1,0:T(8,128)S(1)} %get-tuple-element.31.s, ...), custom_call_target="tpu_custom_call" | custom-call | flops 805306368 | bytes 4194304 | tf_op jit(solution)/shard_map/pallas_call | solution.py:671
